TPU v7x, 512 devices: a 4x2x32 block of a 4x8x32 slice. The times are simulated.
512 devices in a mesh: grp: 2 (over y), sp: 32 (over z), tp: 8 (over x, core).
Axes of the slice: x: 4, y: 2, z: 32, core: 2. Of those that a mesh axis runs over, the one named last changes fastest.
The devices are a block of a 4x8x32 slice.
Arguments:
- query_rows: bfloat16 [24576, 2048], P(('grp', 'sp'), 'tp'), parts along dimension 0, may hold values from -6 to 6, as said below
- key_rows: bfloat16 [24576, 1024], P(('grp', 'sp'), 'tp'), parts along dimension 0, may hold values from -6 to 6, as said below
- value_rows: bfloat16 [24576, 1024], P(('grp', 'sp'), 'tp'), parts along dimension 0, may hold values from -15 to 15
- pool_input: bfloat16 [24576, 2048], P(('grp', 'sp'), 'tp'), parts along dimension 0, may hold values from -6 to 6
- log_gate_sums: float32 [24576, 16], P(('grp', 'sp'), 'tp'), parts along dimension 0, as said below
- query_gain: float32 [128], replicated, may hold values from 0.7 to 4.5, as said below
- key_gain: float32 [128], replicated, may hold values from 0.7 to 4.5, as said below
- pool_weight: bfloat16 [8, 256, 256], P('tp'), may hold values from -0.375 to 0.375
- pool_scale: float32 [2048], P('tp'), may hold values from 0.1 to 1.9
- attention_out: bfloat16 [2048, 4096], P('tp'), may hold values from -0.09375 to 0.09375
- pooling_out: bfloat16 [2048, 4096], P('tp'), may hold values from -0.09375 to 0.09375
Outputs:
- mixed_rows: bfloat16 [24576, 4096], P(('grp', 'sp', 'tp')), parts along dimension 0
There are 2 independent parts, one for each index of `grp`. A program takes and returns all parts, laid end to end along the dimension named above; an argument that names none is the same for every part. Nothing has to cross between parts.
Inputs may be any that keep to these rules, and one draw needn't show every extreme that they name: `query_rows`: normal entries; in some rows a query head's entries may equal its key head's entries of an earlier position. `key_rows`: normal entries. `log_gate_sums`: each column never rises from one position to the next. `query_gain`: Positive. `key_gain`: Positive.
All inputs are finite; a program needn't handle non-finite values.
Results may differ from a plain program's by a relative error of at most 0.014.
The roundings to bfloat16 on the way count: a program that leaves them out, or rounds other values in their place, can miss the bound.
Values may be sent and summed in bfloat16 or wider, within the bound.
A program may use at most 64 MiB of HBM per device.

v0:
```python
import math

import jax
import jax.numpy as jnp
from jax import lax
from jax.sharding import PartitionSpec as P

HEAD = 128
QUERY_HEADS = 16
KV_HEADS = 8
GROUP = 256
MAX_WINDOW = 16


epsilon = 1e-06
masked = -1e30


def from_behind(block, axis, distance):
    devices = range(lax.axis_size(axis))
    route = [(i - distance, i) for i in devices if i - distance in devices]
    return lax.ppermute(block, axis, route)


def split_up(array, dim, devices):
    dims = array.shape
    tiles = array.reshape(*dims[:dim], devices, dims[dim] // devices, *dims[dim + 1 :])
    return jnp.moveaxis(tiles, dim, 0)


def sent_and_summed(array, axis, dim):
    tiles = split_up(array, dim, lax.axis_size(axis))
    arrived = lax.all_to_all(tiles, axis, split_axis=0, concat_axis=0, tiled=True)
    return arrived.astype(jnp.float32).sum(axis=0)


def head_norm(row_data, gain_vector, head_count):
    shaped = row_data.astype(jnp.float32).reshape(row_data.shape[0], head_count, -1)
    scaled = shaped * lax.rsqrt(jnp.mean(shaped * shaped, axis=-1, keepdims=True) + epsilon)
    return (scaled * gain_vector).astype(jnp.bfloat16)


def window_means(padded, length, first_pos, windows):
    rim_rows = padded.shape[0] - length
    window_sum = jnp.zeros((length,) + padded.shape[1:], jnp.float32)
    pooled = window_sum
    for lookback in range(rim_rows + 1):
        window_sum = window_sum + padded[rim_rows - lookback : rim_rows - lookback + length]
        window_size = lookback + 1
        if window_size >= 2 and window_size & window_size - 1 == 0:
            pooled = jnp.where((windows == window_size)[None, :, None], window_sum, pooled)
    positions = (first_pos + jnp.arange(length, dtype=jnp.int32)).astype(jnp.float32)
    counts = jnp.minimum(positions[:, None, None] + 1.0, windows.astype(jnp.float32)[None, :, None])
    return pooled / counts - padded[rim_rows:]


def attend_block(running, queries, query_gates, query_pos, pair_block, key_gates, key_pos):
    row_best, weight_sum, accumulated = running
    scores = jnp.einsum(
        "tkrd,skd->krts", queries, pair_block[0], preferred_element_type=jnp.float32
    )
    scores = scores * (1.0 / math.sqrt(HEAD)) + query_gates - key_gates
    allowed = key_pos[None, :] <= query_pos[:, None]
    scores = jnp.where(allowed, scores, masked)
    new_best = jnp.maximum(row_best, jnp.max(scores, axis=-1, keepdims=True))
    weights = jnp.where(allowed, jnp.exp(scores - new_best), 0.0)
    fading = jnp.exp(row_best - new_best)
    weight_sum = weight_sum * fading + jnp.sum(weights, axis=-1, keepdims=True)
    summed = jnp.einsum(
        "krts,skd->krtd",
        weights.astype(jnp.bfloat16),
        pair_block[1],
        preferred_element_type=jnp.float32,
    )
    return (new_best, weight_sum, accumulated * fading + summed)


def attend_piece(running, piece, queries, query_gates, query_pos, all_gates, valid):
    kv_here = queries.shape[1]
    ratio = queries.shape[2]
    piece_rows = piece.shape[1]
    block_rows = piece_rows
    while block_rows > 1024 and block_rows % 2 == 0:
        block_rows = block_rows // 2
    last_query = query_pos[query_pos.shape[0] - 1]

    def one_block(block_index, loop_state):
        first = block_index * block_rows

        def compute(state):
            pair_block = lax.dynamic_slice_in_dim(piece, block_index * block_rows, block_rows, 1)
            gate_block = lax.dynamic_slice_in_dim(all_gates, jnp.maximum(first, 0), block_rows, 0)
            gate_block = gate_block.T.reshape(kv_here, ratio, 1, block_rows)
            key_pos = first + jnp.arange(block_rows, dtype=jnp.int32)
            return attend_block(
                state, queries, query_gates, query_pos, pair_block, gate_block, key_pos
            )

        needed = jnp.logical_and(valid, first <= last_query)
        return lax.cond(needed, compute, lambda state: state, loop_state)

    return lax.fori_loop(0, piece_rows // block_rows, one_block, running)


def body(
    query_rows,
    key_rows,
    value_rows,
    pool_input,
    log_gate_sums,
    query_gain,
    key_gain,
    pool_weight,
    pool_scale,
    attention_out,
    pooling_out,
):
    length = query_rows.shape[0]
    kv_here = key_rows.shape[1] // HEAD
    ratio = QUERY_HEADS // KV_HEADS
    sp_index = lax.axis_index("sp")
    queries = head_norm(query_rows, query_gain, kv_here * ratio).reshape(
        length, kv_here, ratio, HEAD
    )
    pair = jnp.stack(
        [head_norm(key_rows, key_gain, kv_here), value_rows.reshape(length, kv_here, HEAD)]
    )
    all_gates = lax.all_gather(log_gate_sums, "sp", axis=0, tiled=True)
    query_gates = log_gate_sums.T.reshape(kv_here, ratio, length, 1)
    query_pos = sp_index * length + jnp.arange(length, dtype=jnp.int32)
    start_state = (
        jnp.full((kv_here, ratio, length, 1), masked, jnp.float32),
        jnp.zeros((kv_here, ratio, length, 1), jnp.float32),
        jnp.zeros((kv_here, ratio, length, HEAD), jnp.float32),
    )
    row_best, weight_sum, accumulated = attend_piece(
        start_state,
        lax.all_gather(pair, "sp", axis=1, tiled=True),
        queries,
        query_gates,
        query_pos,
        all_gates,
        jnp.int32(0) >= 0,
    )
    attended = (
        (accumulated / weight_sum)
        .transpose(2, 0, 1, 3)
        .reshape(length, kv_here * ratio * HEAD)
        .astype(jnp.bfloat16)
    )
    group_here = pool_input.shape[1] // GROUP
    rim = from_behind(pool_input[length - (MAX_WINDOW - 1) :], "sp", 1)
    padded = (
        jnp.concatenate([rim, pool_input])
        .astype(jnp.float32)
        .reshape(length + MAX_WINDOW - 1, group_here, GROUP)
    )
    levels = MAX_WINDOW.bit_length() - 1
    groups = lax.axis_index("tp") * group_here + jnp.arange(group_here, dtype=jnp.int32)
    windows = 2 ** (1 + groups % levels)
    pooled = window_means(padded, length, sp_index * length, windows).astype(jnp.bfloat16)
    mixing = jnp.einsum("tgc,gcd->tgd", pooled, pool_weight, preferred_element_type=jnp.float32)
    pool_mixed = (
        (mixing * pool_scale.reshape(group_here, GROUP))
        .astype(jnp.bfloat16)
        .reshape(length, group_here * GROUP)
    )
    total = jnp.dot(attended, attention_out, preferred_element_type=jnp.float32)
    merged = sent_and_summed(
        (total + jnp.dot(pool_mixed, pooling_out, preferred_element_type=jnp.float32)).astype(
            jnp.bfloat16
        ),
        "tp",
        0,
    )
    return merged.astype(jnp.bfloat16)


def solution(mesh):
    return jax.shard_map(
        body,
        mesh=mesh,
        in_specs=(
            P(("grp", "sp"), "tp"),
            P(("grp", "sp"), "tp"),
            P(("grp", "sp"), "tp"),
            P(("grp", "sp"), "tp"),
            P(("grp", "sp"), "tp"),
            P(),
            P(),
            P("tp", None, None),
            P("tp"),
            P("tp", None),
            P("tp", None),
        ),
        out_specs=P(("grp", "sp", "tp"), None),
        check_vma=False,
    )
```

profile of v0, /device:TPU:1952, one launch (start us, length us, event | category | flops | bytes accessed | tf_op | source)
XLA Modules:
  0.0 316.9 jit_solution(8396931143499803116)
XLA Ops:
  8.8 1.6 pad_maximum_fusion
  11.1 3.8 %collective-permute-start = (bf16[15,256]{1,0:T(8,128)(2,1)S(1)}, bf16[15,256]{1,0:T(8,128)(2,1)S(1)}, u32[]{:S(2)}, u32[]{:S(2)}) collective-permute-start(bf16[15,256]{1,0:T(8,128)(2,1)S(1)} %slice.78), channel_id=1, source_target_pairs={{0,8},{8,16},{16,24},{24,32},{32,40},{40,48},{48,56},{56,64},{64,7... | collective-permute-start | bytes 23048 | tf_op jit(solution)/shard_map/ppermute | solution.py:22
  17.0 51.1 %all_gather.7 = f32[12288,2]{0,1:T(2,128)S(1)} all-gather(f32[384,2]{0,1:T(2,128)} %param.19), channel_id=1, replica_groups=mesh['grp'=2,'sp'=32,'tp'=8] {'sp'}, dimensions={0}, use_global_device_ids=true | all-gather | bytes 101376 | tf_op jit(solution)/shard_map/all_gather | solution.py:128
  69.7 71.2 %all-gather.2.cloned.1.call-done = bf16[2,12288,1,128]{3,1,2,0:T(8,128)(2,1)} async-done(((bf16[2,384,1,128]{3,1,2,0:T(8,128)(2,1)}), bf16[2,12288,1,128]{3,1,2,0:T(8,128)(2,1)}) %all-gather.2.cloned.1.call-update) | async-done | bytes 6291472 | tf_op jit(solution)/shard_map/all_gather | solution.py:138
  141.0 113.0 %while.18 = (s32[]{:T(128)}, f32[1,2,384,1]{2,1,3,0:T(2,128)S(1)}, f32[1,2,384,1]{2,1,3,0:T(2,128)S(1)}, f32[1,2,384,128]{3,2,1,0:T(8,128)S(1)}, s32[]{:T(128)},...) while((s32[]{:T(128)}, f32[1,2,384,1]{2,1,3,0:T(2,128)S(1)}, ...), condition=%wide.region_7.8_spmd.clone, body=%wide.region_2.7_spmd.clone.sunk | while | flops 308972928 | bytes 19154336 | solution.py:102
  141.6 6.4 %conditional.3 = ((f32[1,2,384,1]{2,1,3,0:T(2,128)S(1)}, f32[1,2,384,1]{2,1,3,0:T(2,128)S(1)}, f32[1,2,384,128]{3,2,1,0:T(8,128)S(1)})) conditional(s32[]{:T(128)} %convert_element_type.116, (f32[1,2,384,1]{2,1,3,0:T(2,128)S(1)}, f32[1,2,384,1]{2,1,3,0:T(2,128)S(1)}, f32[1,2,384,128]{3,2,1,0:T(8,128)S(1)}) %tuple.45, (s32[]{:T(128)}, s32[]{:T(128)}, ...), branch_computations={%region_3.0_spmd, %region_4.6_spmd} | conditional | flops 308972928 | bytes 19152538 | solution.py:100
  141.9 1.7 fusion.47
  143.6 1.4 copy-done.1
  145.6 2.4 fusion.6
  148.7 6.4 %conditional.3 = ((f32[1,2,384,1]{2,1,3,0:T(2,128)S(1)}, f32[1,2,384,1]{2,1,3,0:T(2,128)S(1)}, f32[1,2,384,128]{3,2,1,0:T(8,128)S(1)})) conditional(s32[]{:T(128)} %convert_element_type.116, (f32[1,2,384,1]{2,1,3,0:T(2,128)S(1)}, f32[1,2,384,1]{2,1,3,0:T(2,128)S(1)}, f32[1,2,384,128]{3,2,1,0:T(8,128)S(1)}) %tuple.45, (s32[]{:T(128)}, s32[]{:T(128)}, ...), branch_computations={%region_3.0_spmd, %region_4.6_spmd} | conditional | flops 308972928 | bytes 19152538 | solution.py:100
  149.0 1.7 fusion.47
  150.7 1.4 copy-done.1
  152.6 2.4 fusion.6
  155.7 6.4 %conditional.3 = ((f32[1,2,384,1]{2,1,3,0:T(2,128)S(1)}, f32[1,2,384,1]{2,1,3,0:T(2,128)S(1)}, f32[1,2,384,128]{3,2,1,0:T(8,128)S(1)})) conditional(s32[]{:T(128)} %convert_element_type.116, (f32[1,2,384,1]{2,1,3,0:T(2,128)S(1)}, f32[1,2,384,1]{2,1,3,0:T(2,128)S(1)}, f32[1,2,384,128]{3,2,1,0:T(8,128)S(1)}) %tuple.45, (s32[]{:T(128)}, s32[]{:T(128)}, ...), branch_computations={%region_3.0_spmd, %region_4.6_spmd} | conditional | flops 308972928 | bytes 19152538 | solution.py:100
  156.1 1.7 fusion.47
  159.7 2.4 fusion.6
  162.8 6.4 %conditional.3 = ((f32[1,2,384,1]{2,1,3,0:T(2,128)S(1)}, f32[1,2,384,1]{2,1,3,0:T(2,128)S(1)}, f32[1,2,384,128]{3,2,1,0:T(8,128)S(1)})) conditional(s32[]{:T(128)} %convert_element_type.116, (f32[1,2,384,1]{2,1,3,0:T(2,128)S(1)}, f32[1,2,384,1]{2,1,3,0:T(2,128)S(1)}, f32[1,2,384,128]{3,2,1,0:T(8,128)S(1)}) %tuple.45, (s32[]{:T(128)}, s32[]{:T(128)}, ...), branch_computations={%region_3.0_spmd, %region_4.6_spmd} | conditional | flops 308972928 | bytes 19152538 | solution.py:100
  163.1 1.7 fusion.47
  164.8 1.4 copy-done.1
  166.8 2.4 fusion.6
  169.9 6.4 %conditional.3 = ((f32[1,2,384,1]{2,1,3,0:T(2,128)S(1)}, f32[1,2,384,1]{2,1,3,0:T(2,128)S(1)}, f32[1,2,384,128]{3,2,1,0:T(8,128)S(1)})) conditional(s32[]{:T(128)} %convert_element_type.116, (f32[1,2,384,1]{2,1,3,0:T(2,128)S(1)}, f32[1,2,384,1]{2,1,3,0:T(2,128)S(1)}, f32[1,2,384,128]{3,2,1,0:T(8,128)S(1)}) %tuple.45, (s32[]{:T(128)}, s32[]{:T(128)}, ...), branch_computations={%region_3.0_spmd, %region_4.6_spmd} | conditional | flops 308972928 | bytes 19152538 | solution.py:100
  170.2 1.7 fusion.47
  171.9 1.4 copy-done.1
  173.8 2.4 fusion.6
  176.9 6.4 %conditional.3 = ((f32[1,2,384,1]{2,1,3,0:T(2,128)S(1)}, f32[1,2,384,1]{2,1,3,0:T(2,128)S(1)}, f32[1,2,384,128]{3,2,1,0:T(8,128)S(1)})) conditional(s32[]{:T(128)} %convert_element_type.116, (f32[1,2,384,1]{2,1,3,0:T(2,128)S(1)}, f32[1,2,384,1]{2,1,3,0:T(2,128)S(1)}, f32[1,2,384,128]{3,2,1,0:T(8,128)S(1)}) %tuple.45, (s32[]{:T(128)}, s32[]{:T(128)}, ...), branch_computations={%region_3.0_spmd, %region_4.6_spmd} | conditional | flops 308972928 | bytes 19152538 | solution.py:100
  177.3 1.7 fusion.47
  180.9 2.4 fusion.6
  184.0 6.4 %conditional.3 = ((f32[1,2,384,1]{2,1,3,0:T(2,128)S(1)}, f32[1,2,384,1]{2,1,3,0:T(2,128)S(1)}, f32[1,2,384,128]{3,2,1,0:T(8,128)S(1)})) conditional(s32[]{:T(128)} %convert_element_type.116, (f32[1,2,384,1]{2,1,3,0:T(2,128)S(1)}, f32[1,2,384,1]{2,1,3,0:T(2,128)S(1)}, f32[1,2,384,128]{3,2,1,0:T(8,128)S(1)}) %tuple.45, (s32[]{:T(128)}, s32[]{:T(128)}, ...), branch_computations={%region_3.0_spmd, %region_4.6_spmd} | conditional | flops 308972928 | bytes 19152538 | solution.py:100
  184.3 1.7 fusion.47
  188.0 2.4 fusion.6
  191.0 6.4 %conditional.3 = ((f32[1,2,384,1]{2,1,3,0:T(2,128)S(1)}, f32[1,2,384,1]{2,1,3,0:T(2,128)S(1)}, f32[1,2,384,128]{3,2,1,0:T(8,128)S(1)})) conditional(s32[]{:T(128)} %convert_element_type.116, (f32[1,2,384,1]{2,1,3,0:T(2,128)S(1)}, f32[1,2,384,1]{2,1,3,0:T(2,128)S(1)}, f32[1,2,384,128]{3,2,1,0:T(8,128)S(1)}) %tuple.45, (s32[]{:T(128)}, s32[]{:T(128)}, ...), branch_computations={%region_3.0_spmd, %region_4.6_spmd} | conditional | flops 308972928 | bytes 19152538 | solution.py:100
  191.4 1.7 fusion.47
  195.0 2.4 fusion.6
  198.1 6.4 %conditional.3 = ((f32[1,2,384,1]{2,1,3,0:T(2,128)S(1)}, f32[1,2,384,1]{2,1,3,0:T(2,128)S(1)}, f32[1,2,384,128]{3,2,1,0:T(8,128)S(1)})) conditional(s32[]{:T(128)} %convert_element_type.116, (f32[1,2,384,1]{2,1,3,0:T(2,128)S(1)}, f32[1,2,384,1]{2,1,3,0:T(2,128)S(1)}, f32[1,2,384,128]{3,2,1,0:T(8,128)S(1)}) %tuple.45, (s32[]{:T(128)}, s32[]{:T(128)}, ...), branch_computations={%region_3.0_spmd, %region_4.6_spmd} | conditional | flops 308972928 | bytes 19152538 | solution.py:100
  198.5 1.7 fusion.47
  202.1 2.4 fusion.6
  205.2 6.4 %conditional.3 = ((f32[1,2,384,1]{2,1,3,0:T(2,128)S(1)}, f32[1,2,384,1]{2,1,3,0:T(2,128)S(1)}, f32[1,2,384,128]{3,2,1,0:T(8,128)S(1)})) conditional(s32[]{:T(128)} %convert_element_type.116, (f32[1,2,384,1]{2,1,3,0:T(2,128)S(1)}, f32[1,2,384,1]{2,1,3,0:T(2,128)S(1)}, f32[1,2,384,128]{3,2,1,0:T(8,128)S(1)}) %tuple.45, (s32[]{:T(128)}, s32[]{:T(128)}, ...), branch_computations={%region_3.0_spmd, %region_4.6_spmd} | conditional | flops 308972928 | bytes 19152538 | solution.py:100
  205.5 1.7 fusion.47
  207.2 1.4 copy-done.1
  209.2 2.4 fusion.6
  212.2 6.4 %conditional.3 = ((f32[1,2,384,1]{2,1,3,0:T(2,128)S(1)}, f32[1,2,384,1]{2,1,3,0:T(2,128)S(1)}, f32[1,2,384,128]{3,2,1,0:T(8,128)S(1)})) conditional(s32[]{:T(128)} %convert_element_type.116, (f32[1,2,384,1]{2,1,3,0:T(2,128)S(1)}, f32[1,2,384,1]{2,1,3,0:T(2,128)S(1)}, f32[1,2,384,128]{3,2,1,0:T(8,128)S(1)}) %tuple.45, (s32[]{:T(128)}, s32[]{:T(128)}, ...), branch_computations={%region_3.0_spmd, %region_4.6_spmd} | conditional | flops 308972928 | bytes 19152538 | solution.py:100
  212.6 1.7 fusion.47
  214.3 1.4 copy-done.1
  216.2 2.4 fusion.6
  219.3 6.4 %conditional.3 = ((f32[1,2,384,1]{2,1,3,0:T(2,128)S(1)}, f32[1,2,384,1]{2,1,3,0:T(2,128)S(1)}, f32[1,2,384,128]{3,2,1,0:T(8,128)S(1)})) conditional(s32[]{:T(128)} %convert_element_type.116, (f32[1,2,384,1]{2,1,3,0:T(2,128)S(1)}, f32[1,2,384,1]{2,1,3,0:T(2,128)S(1)}, f32[1,2,384,128]{3,2,1,0:T(8,128)S(1)}) %tuple.45, (s32[]{:T(128)}, s32[]{:T(128)}, ...), branch_computations={%region_3.0_spmd, %region_4.6_spmd} | conditional | flops 308972928 | bytes 19152538 | solution.py:100
  219.7 1.7 fusion.47
  223.3 2.4 fusion.6
  226.4 6.4 %conditional.3 = ((f32[1,2,384,1]{2,1,3,0:T(2,128)S(1)}, f32[1,2,384,1]{2,1,3,0:T(2,128)S(1)}, f32[1,2,384,128]{3,2,1,0:T(8,128)S(1)})) conditional(s32[]{:T(128)} %convert_element_type.116, (f32[1,2,384,1]{2,1,3,0:T(2,128)S(1)}, f32[1,2,384,1]{2,1,3,0:T(2,128)S(1)}, f32[1,2,384,128]{3,2,1,0:T(8,128)S(1)}) %tuple.45, (s32[]{:T(128)}, s32[]{:T(128)}, ...), branch_computations={%region_3.0_spmd, %region_4.6_spmd} | conditional | flops 308972928 | bytes 19152538 | solution.py:100
  226.7 1.7 fusion.47
  230.4 2.4 fusion.6
  233.4 6.4 %conditional.3 = ((f32[1,2,384,1]{2,1,3,0:T(2,128)S(1)}, f32[1,2,384,1]{2,1,3,0:T(2,128)S(1)}, f32[1,2,384,128]{3,2,1,0:T(8,128)S(1)})) conditional(s32[]{:T(128)} %convert_element_type.116, (f32[1,2,384,1]{2,1,3,0:T(2,128)S(1)}, f32[1,2,384,1]{2,1,3,0:T(2,128)S(1)}, f32[1,2,384,128]{3,2,1,0:T(8,128)S(1)}) %tuple.45, (s32[]{:T(128)}, s32[]{:T(128)}, ...), branch_computations={%region_3.0_spmd, %region_4.6_spmd} | conditional | flops 308972928 | bytes 19152538 | solution.py:100
  233.8 1.7 fusion.47
  237.4 2.4 fusion.6
  240.5 6.4 %conditional.3 = ((f32[1,2,384,1]{2,1,3,0:T(2,128)S(1)}, f32[1,2,384,1]{2,1,3,0:T(2,128)S(1)}, f32[1,2,384,128]{3,2,1,0:T(8,128)S(1)})) conditional(s32[]{:T(128)} %convert_element_type.116, (f32[1,2,384,1]{2,1,3,0:T(2,128)S(1)}, f32[1,2,384,1]{2,1,3,0:T(2,128)S(1)}, f32[1,2,384,128]{3,2,1,0:T(8,128)S(1)}) %tuple.45, (s32[]{:T(128)}, s32[]{:T(128)}, ...), branch_computations={%region_3.0_spmd, %region_4.6_spmd} | conditional | flops 308972928 | bytes 19152538 | solution.py:100
  240.9 1.7 fusion.47
  244.5 2.4 fusion.6
  247.6 6.4 %conditional.3 = ((f32[1,2,384,1]{2,1,3,0:T(2,128)S(1)}, f32[1,2,384,1]{2,1,3,0:T(2,128)S(1)}, f32[1,2,384,128]{3,2,1,0:T(8,128)S(1)})) conditional(s32[]{:T(128)} %convert_element_type.116, (f32[1,2,384,1]{2,1,3,0:T(2,128)S(1)}, f32[1,2,384,1]{2,1,3,0:T(2,128)S(1)}, f32[1,2,384,128]{3,2,1,0:T(8,128)S(1)}) %tuple.45, (s32[]{:T(128)}, s32[]{:T(128)}, ...), branch_computations={%region_3.0_spmd, %region_4.6_spmd} | conditional | flops 308972928 | bytes 19152538 | solution.py:100
  247.9 1.7 fusion.47
  249.6 1.4 copy-done.1
  251.6 2.4 fusion.6
  254.3 3.7 %fusion.48 = f32[384,4096]{1,0:T(8,128)} fusion(bf16[384,256]{0,1:T(8,128)(2,1)S(1)} %bitcast.94, bf16[256,4096]{1,0:T(8,128)(2,1)S(1)} %copy-done), kind=kOutput, calls=%fused_computation.77 | convolution fusion | flops 805306368 | bytes 8585216 | tf_op jit(solution)/shard_map/dot_general | solution.py:168
  257.9 5.9 %add_convert_fusion = bf16[384,4096]{1,0:T(8,128)(2,1)} fusion(f32[384,4096]{1,0:T(8,128)} %fusion.48, bf16[256,4096]{1,0:T(8,128)(2,1)} %param.25, f32[399,256]{1,0:T(8,128)S(1)} %copy-done.2, f32[256]{0:T(256)S(1)} %copy-done.6, f32[384]{0:T(512)S(1)} %add_minimum_fusion, pred[]{:T(512)} %bitcast.29, pred[]{:T(512)} %bitcast.28, pred[]{:T(512)} %bitcast.27, ...), kind=kOutput, calls=%fused_computation.27 | convolution fusion | flops 861143040 | bytes 17959940 | tf_op jit(solution)/shard_map/dot_general | solution.py:170
  263.9 43.0 %all_to_all.5 = bf16[8,48,4096]{2,1,0:T(8,128)(2,1)} all-to-all(bf16[8,48,4096]{2,1,0:T(8,128)(2,1)} %bitcast.90), channel_id=1, replica_groups=mesh['grp'=2,'sp'=32,'tp'=8] {'tp'}, dimensions={0} | all-to-all | bytes 6291456 | tf_op jit(solution)/shard_map/all_to_all | solution.py:33
  306.8 3.2 %reduce_sum.41 = bf16[48,4096]{1,0:T(8,128)(2,1)} reduce(bf16[8,48,4096]{2,1,0:T(8,128)(2,1)} %all_to_all.5, bf16[]{:T(256)} %constant.106.clone.1), dimensions={0}, to_apply=%region_8.9 | reduce | flops 1376256 | bytes 3538946 | tf_op jit(solution)/shard_map/reduce_sum | solution.py:34
  (202 shorter events, 32.7 us)
Async XLA Ops:
  6.5 247.7 %copy-start = (bf16[256,4096]{1,0:T(8,128)(2,1)S(1)}, bf16[256,4096]{1,0:T(8,128)(2,1)}, u32[]{:S(2)}) copy-start(bf16[256,4096]{1,0:T(8,128)(2,1)} %param.24) | copy-start | bytes 6291460
  6.6 62.3 %copy-start.3 = (bf16[384,256]{1,0:T(8,128)(2,1)S(1)}, bf16[384,256]{1,0:T(8,128)(2,1)}, u32[]{:S(2)}) copy-start(bf16[384,256]{1,0:T(8,128)(2,1)} %param.18) | copy-start | bytes 589828
  6.6 134.4 %copy-start.4 = (f32[384,2]{0,1:T(2,128)S(1)}, f32[384,2]{0,1:T(2,128)}, u32[]{:S(2)}) copy-start(f32[384,2]{0,1:T(2,128)} %param.19) | copy-start | bytes 9220
  6.6 134.4 %all-gather.2.cloned.1.call-start = ((), (), s32[]{:S(2)}) async-start(), calls=%async_computation.1 | async-start | bytes 6488064 | tf_op jit(solution)/shard_map/all_gather | solution.py:138
  11.1 57.7 %collective-permute-start = (bf16[15,256]{1,0:T(8,128)(2,1)S(1)}, bf16[15,256]{1,0:T(8,128)(2,1)S(1)}, u32[]{:S(2)}, u32[]{:S(2)}) collective-permute-start(bf16[15,256]{1,0:T(8,128)(2,1)S(1)} %slice.78), channel_id=1, source_target_pairs={{0,8},{8,16},{16,24},{24,32},{32,40},{40,48},{48,56},{56,64},{64,7... | collective-permute-start | bytes 23048 | tf_op jit(solution)/shard_map/ppermute | solution.py:22
  143.6 1.4 copy-start.1
  150.7 1.4 copy-start.1
  157.8 1.4 copy-start.1
  164.8 1.4 copy-start.1
  171.9 1.4 copy-start.1
  179.0 1.4 copy-start.1
  186.0 1.4 copy-start.1
  193.1 1.4 copy-start.1
  200.1 1.4 copy-start.1
  207.2 1.4 copy-start.1
  214.3 1.4 copy-start.1
  221.3 1.4 copy-start.1
  228.4 1.4 copy-start.1
  235.5 1.4 copy-start.1
  242.5 1.4 copy-start.1
  249.6 1.4 copy-start.1
  254.2 3.7 %copy-start.2 = (f32[399,256]{1,0:T(8,128)S(1)}, f32[399,256]{1,0:T(8,128)}, u32[]{:S(2)}) copy-start(f32[399,256]{1,0:T(8,128)} %maximum_convert_fusion) | copy-start | bytes 1225732
  254.2 3.7 %copy-start.5 = (bf16[1,256,256]{2,1,0:T(8,128)(2,1)S(1)}, bf16[1,256,256]{2,1,0:T(8,128)(2,1)}, u32[]{:S(2)}) copy-start(bf16[1,256,256]{2,1,0:T(8,128)(2,1)} %param.22) | copy-start | bytes 393220
  254.3 3.7 %copy-start.6 = (f32[256]{0:T(256)S(1)}, f32[256]{0:T(256)}, u32[]{:S(2)}) copy-start(f32[256]{0:T(256)} %param.23) | copy-start | bytes 3076
Sparse Core Ops, SparseCore 0:
  10.6 130.3 all-gather.1
where the time goes:
time: 318 us; the launch traced here: 317 us
  blocking collectives  94.1 us (30%)
  matrix products  75.5 us (24%)
  waiting for transfers between devices  71.2 us (22%)
  local copies, waits for them, and re-layouts  26.8 us (8%)
  other arithmetic  20.6 us (6%)
  between operations  13.6 us (4%)
  loops' own time  11.4 us (4%)
  starting transfers between devices  3.81 us (1%)
    all_gather x1, waiting for transfers between devices, body(): lax.all_gather(pair, 'sp', axis=1, tiled=True)  71.2 us
    all_gather x1, blocking collectives, body(): all_gates = lax.all_gather(log_gate_sums, 'sp', axis=0, tiled=True)  51.1 us
    all_to_all x1, blocking collectives, sent_and_summed(): lax.all_to_all(tiles, axis, split_axis=0, concat_axis=0, tiled=True)  43 us
    dot_general x16, matrix products, attend_block(): jnp.einsum('krts,skd->krtd', weights.astype(jnp.bfloat16), pair_block[1],...  38.9 us
    dot_general x16, matrix products, attend_block(): jnp.einsum('tkrd,skd->krts', queries, pair_block[0], preferred_element_ty...  27 us
    cond x48, local copies, waits for them, and re-layouts  22.7 us
    another operation x1, loops' own time, attend_piece(): return lax.fori_loop(0, piece_rows // block_rows, one_block, running)  10.3 us
    reduce_sum x16, other arithmetic, attend_block(): weight_sum = weight_sum * fading + jnp.sum(weights, axis=-1, keepdims=True)  7.76 us
  transfers between devices with their start and end apart: 2, of which 1 were waited for; matrix products, arithmetic and copies ran while one was open for 1% of the time, Pallas kernels for 0%

commit v1 on v0

v1 whole, which is shorter than its diff:
```python
import functools
import math

import jax
import jax.numpy as jnp
from jax import lax
from jax.experimental import pallas as pl
from jax.experimental.pallas import tpu as pltpu
from jax.sharding import PartitionSpec as P

HEAD = 128
MAX_WINDOW = 16
LANES = 128
CHUNKS = 4

epsilon = 1e-06
masked = -1e30
LOG2E = math.log2(math.e)

f32 = jnp.float32
bf16 = jnp.bfloat16


def normed(rows, gain):
    wide = rows.astype(f32)
    scale = lax.rsqrt(jnp.mean(wide * wide, axis=-1, keepdims=True) + epsilon)
    return (wide * scale * gain).astype(bf16)


def rows_dot(a, b):
    return lax.dot_general(a, b, (((1,), (1,)), ((), ())), preferred_element_type=f32)


def dot(a, b):
    return jnp.dot(a, b, preferred_element_type=f32)


def kernel(
    n_sp,
    n_tp,
    q_ref,
    k_ref,
    v_ref,
    gate_ref,
    pool_ref,
    q_gain_ref,
    k_gain_ref,
    pool_w_ref,
    pool_s_ref,
    att_w_hbm,
    pool_w_out_hbm,
    out_ref,
    keys,
    values,
    gates,
    queries,
    best,
    total,
    acc,
    mix,
    rim,
    w_att,
    w_pool,
    pool_part,
    parts,
    relay,
    landed,
    up_send,
    up_recv,
    down_send,
    down_recv,
    early_send,
    early_recv,
    local_sem,
    mix_send,
    mix_recv,
    relay_send,
    relay_recv,
    land_send,
    land_recv,
):
    me = lax.axis_index("sp")
    tp = lax.axis_index("tp")
    length = q_ref.shape[0]
    heads = q_ref.shape[1] // HEAD
    pieces = length // LANES
    n_x = n_tp // 2
    core = lax.rem(tp, 2)
    other = 1 - core
    chip = tp // 2
    chip_right = lax.rem(chip + 1, n_x)
    chip_left = lax.rem(chip + n_x - 1, n_x)
    chip_far = lax.rem(chip + 2, n_x)
    above = lax.rem(me + 1, n_sp)
    below = lax.rem(me + n_sp - 1, n_sp)
    n_up = n_sp // 2
    n_down = n_sp - 1 - n_up
    half = out_ref.shape[1] // 2
    cols = half // CHUNKS
    rows = out_ref.shape[0]

    def remote(src, dst, send_sem, recv_sem, **where):
        return pltpu.make_async_remote_copy(
            src_ref=src,
            dst_ref=dst,
            send_sem=send_sem,
            recv_sem=recv_sem,
            device_id=where,
            device_id_type=pl.DeviceIdType.MESH,
        )

    barrier = pltpu.get_barrier_semaphore()
    for where in (
        {"sp": above},
        {"sp": below},
        {"tp": 2 * chip + other},
        {"tp": 2 * chip_right},
        {"tp": 2 * chip_right + 1},
        {"tp": 2 * chip_left},
        {"tp": 2 * chip_left + 1},
    ):
        pl.semaphore_signal(
            barrier, inc=1, device_id=where, device_id_type=pl.DeviceIdType.MESH
        )

    my_cols = pl.ds(pl.multiple_of(core * half, LANES), half)
    other_cols = pl.ds(pl.multiple_of(other * half, LANES), half)
    load_att = pltpu.make_async_copy(att_w_hbm.at[:, my_cols], w_att.at[0], local_sem.at[0])
    load_pool = pltpu.make_async_copy(
        pool_w_out_hbm.at[:, my_cols], w_pool.at[0], local_sem.at[1]
    )
    load_att.start()
    load_pool.start()

    keys[me] = normed(k_ref[...], k_gain_ref[...])
    values[me] = v_ref[...]
    gates[me] = gate_ref[...]

    pl.semaphore_wait(barrier, 7)

    def ring_copies(slot, step, src_first):
        sources = (
            (v_ref, gate_ref, keys.at[slot])
            if src_first
            else (values.at[slot], gates.at[slot], keys.at[slot])
        )
        targets = (values.at[slot], gates.at[slot], keys.at[slot])
        return sources, targets

    def up_copy(kind, slot, step, src_first=False):
        sources, targets = ring_copies(slot, step, src_first)
        return remote(
            sources[kind],
            targets[kind],
            up_send.at[kind, step],
            up_recv.at[kind, step],
            sp=above,
        )

    def down_copy(kind, slot, step, src_first=False):
        sources, targets = ring_copies(slot, step, src_first)
        return remote(
            sources[kind],
            targets[kind],
            down_send.at[kind, step],
            down_recv.at[kind, step],
            sp=below,
        )

    for kind in (0, 1):
        up_copy(kind, me, 0, True).start()
        if n_down > 0:
            down_copy(kind, me, 0, True).start()
    for h in range(heads):
        queries[h] = normed(q_ref[:, h * HEAD : (h + 1) * HEAD], q_gain_ref[...])
    up_copy(2, me, 0, True).start()
    if n_down > 0:
        down_copy(2, me, 0, True).start()

    rim_copy = remote(
        pool_ref.at[pl.ds(length - MAX_WINDOW, MAX_WINDOW)],
        rim,
        early_send.at[0],
        early_recv.at[0],
        sp=above,
    )
    att_w_copy = remote(
        att_w_hbm.at[:, other_cols],
        w_att.at[1],
        early_send.at[1],
        early_recv.at[1],
        tp=2 * chip + other,
    )
    pool_w_copy = remote(
        pool_w_out_hbm.at[:, other_cols],
        w_pool.at[1],
        early_send.at[2],
        early_recv.at[2],
        tp=2 * chip + other,
    )
    rim_copy.start()
    att_w_copy.start()
    pool_w_copy.start()

    scale = LOG2E / math.sqrt(HEAD)

    def score_pieces(h, slot):
        z = rows_dot(queries[h], keys[slot])
        base = gate_ref[h * pieces : h * pieces + 1, 0:1]
        lifted = (base - gates[slot]) * LOG2E
        return [
            z[:, c * LANES : (c + 1) * LANES] * scale
            + lifted[h * pieces + c : h * pieces + c + 1, :]
            for c in range(pieces)
        ]

    def row_max(score):
        most = functools.reduce(jnp.maximum, score)
        return jnp.max(most, axis=-1, keepdims=True)

    def weigh(score, top):
        weights = [jnp.exp2(s - top) for s in score]
        return functools.reduce(jnp.add, weights), jnp.concatenate(
            [w.astype(bf16) for w in weights], axis=1
        )

    def attend_own():
        for h in range(heads):
            score = score_pieces(h, me)
            position = lax.broadcasted_iota(jnp.int32, (length, LANES), 0)
            lane = lax.broadcasted_iota(jnp.int32, (length, LANES), 1)
            score = [
                jnp.where(lane + c * LANES <= position, s, masked) for c, s in enumerate(score)
            ]
            top = jnp.broadcast_to(row_max(score), (length, LANES))
            summed, weights = weigh(score, top)
            best[h] = top
            total[h] = summed
            acc[h] = dot(weights, values[me])

    def attend(slot):
        for h in range(heads):
            score = score_pieces(h, slot)
            before = best[h]
            top = jnp.maximum(before, row_max(score))
            fade = jnp.exp2(before - top)
            summed, weights = weigh(score, top)
            best[h] = top
            total[h] = total[h] * fade + summed
            acc[h] = acc[h] * fade + dot(weights, values[slot])

    attend_own()

    level_count = MAX_WINDOW.bit_length() - 1
    level = lax.rem(tp, level_count)

    def pooling():
        rim_copy.wait_recv()
        edge = jnp.where(me > 0, rim[...].astype(f32), 0.0)
        here = pool_ref[...].astype(f32)
        window_sum = jnp.concatenate([edge, here], axis=0)
        chosen = jnp.zeros_like(here)
        for k in range(level_count):
            window_sum = window_sum + pltpu.roll(window_sum, 1 << k, 0)
            chosen = jnp.where(level == k, window_sum[MAX_WINDOW:], chosen)
        window = (2 << level).astype(f32) if hasattr(level, "astype") else float(2 << level)
        position = me * length + lax.broadcasted_iota(jnp.int32, here.shape, 0)
        counts = jnp.minimum(position.astype(f32) + 1.0, window)
        pooled = (chosen / counts - here).astype(bf16)
        mixed = dot(pooled, pool_w_ref[0]) * pool_s_ref[...]
        mix[0] = mixed.astype(bf16)

    pooling()
    partner = 2 * chip + other
    pool_mix_copy = remote(
        mix.at[0], mix.at[1], mix_send.at[0], mix_recv.at[0], tp=partner
    )

    def ring_step(step, carry):
        slot_up = lax.rem(me - step + n_sp, n_sp)
        slot_down = lax.rem(me + step, n_sp)
        for kind in range(3):
            up_copy(kind, slot_up, step - 1).wait_recv()

            @pl.when(step < n_up)
            def _():
                up_copy(kind, slot_up, step).start()

            if n_down > 0:

                @pl.when(step <= n_down)
                def _():
                    down_copy(kind, slot_down, step - 1).wait_recv()

                @pl.when(step < n_down)
                def _():
                    down_copy(kind, slot_down, step).start()

        @pl.when(step <= me)
        def _():
            attend(slot_up)

        @pl.when(jnp.logical_and(step <= n_down, me + step >= n_sp))
        def _():
            attend(slot_down)

        return carry

    lax.fori_loop(1, 2, ring_step, 0)

    pool_mix_copy.start()
    load_att.wait()
    load_pool.wait()
    att_w_copy.wait_recv()
    pool_w_copy.wait_recv()
    pool_mix_copy.wait_recv()
    for c in range(CHUNKS):
        span = pl.ds(c * cols, cols)
        pool_part[:, span] = dot(mix[0], w_pool[0, :, span]) + dot(mix[1], w_pool[1, :, span])

    lax.fori_loop(2, n_up + 1, ring_step, 0)

    for h in range(heads):
        weight_sum = jnp.sum(total[h], axis=-1, keepdims=True)
        mix[2, :, h * HEAD : (h + 1) * HEAD] = (acc[h] / weight_sum).astype(bf16)
    att_mix_copy = remote(mix.at[2], mix.at[3], mix_send.at[1], mix_recv.at[1], tp=partner)
    att_mix_copy.start()
    att_mix_copy.wait_recv()

    def relay_copies(c):
        return (
            remote(
                parts.at[2 * chip_far, c],
                relay.at[0, c],
                relay_send.at[0, c],
                relay_recv.at[0, c],
                tp=2 * chip_right + core,
            ),
            remote(
                parts.at[2 * chip_far + 1, c],
                relay.at[1, c],
                relay_send.at[1, c],
                relay_recv.at[1, c],
                tp=2 * chip_left + core,
            ),
        )

    def land_copy(side, target_chip, target_core, c):
        target = 2 * target_chip + target_core
        return remote(
            parts.at[target, c],
            landed.at[side, core, c],
            land_send.at[side, target_core, c],
            land_recv.at[side, core, c],
            tp=target,
        )

    def home_copy(c):
        return remote(
            parts.at[partner, c],
            landed.at[2, core, c],
            land_send.at[2, 0, c],
            land_recv.at[2, core, c],
            tp=partner,
        )

    for c in range(CHUNKS):
        span = pl.ds(c * cols, cols)
        part = (
            dot(mix[2], w_att[0, :, span])
            + dot(mix[3], w_att[1, :, span])
            + pool_part[:, span]
        ).astype(bf16)
        for d in range(n_tp):
            parts[d, c] = part[d * rows : (d + 1) * rows]
        for copy in relay_copies(c):
            copy.start()
    for c in range(CHUNKS):
        land_copy(0, chip_right, 1, c).start()
        land_copy(1, chip_left, 0, c).start()
    for c in range(CHUNKS):
        home_copy(c).start()
    for c in range(CHUNKS):
        from_left, from_right = relay_copies(c)
        for side, copy, target in (
            (0, from_left, 2 * chip_right),
            (1, from_right, 2 * chip_left + 1),
        ):
            copy.wait_recv()
            joined = parts[target, c].astype(f32) + relay[side, c].astype(f32)
            parts[target, c] = joined.astype(bf16)
        land_copy(0, chip_right, 0, c).start()
        land_copy(1, chip_left, 1, c).start()

    def landed_wait(side, source_core, c):
        remote(
            landed.at[side, source_core, c],
            landed.at[side, source_core, c],
            land_send.at[side, 0, c],
            land_recv.at[side, source_core, c],
            tp=partner,
        ).wait_recv()

    for c in range(CHUNKS):
        landed_wait(2, other, c)
        for source_core in range(2):
            landed_wait(0, source_core, c)
            landed_wait(1, source_core, c)
        for source_core in range(2):
            home = jnp.where(
                core == source_core,
                parts[tp, c].astype(f32),
                landed[2, source_core, c].astype(f32),
            )
            merged = (
                home
                + landed[0, source_core, c].astype(f32)
                + landed[1, source_core, c].astype(f32)
            )
            first = source_core * half + c * cols
            out_ref[:, first : first + cols] = merged.astype(bf16)

    def sent(step, carry):
        for kind in range(3):
            up_copy(kind, me, step).wait_send()
            if n_down > 0:

                @pl.when(step < n_down)
                def _():
                    down_copy(kind, me, step).wait_send()

        return carry

    lax.fori_loop(0, n_up, sent, 0)
    rim_copy.wait_send()
    att_w_copy.wait_send()
    pool_w_copy.wait_send()
    pool_mix_copy.wait_send()
    att_mix_copy.wait_send()
    for c in range(CHUNKS):
        for copy in relay_copies(c):
            copy.wait_send()
        land_copy(0, chip_right, 1, c).wait_send()
        land_copy(1, chip_left, 0, c).wait_send()
        land_copy(0, chip_right, 0, c).wait_send()
        land_copy(1, chip_left, 1, c).wait_send()
        home_copy(c).wait_send()


def body(
    n_sp,
    n_tp,
    query_rows,
    key_rows,
    value_rows,
    pool_input,
    log_gate_sums,
    query_gain,
    key_gain,
    pool_weight,
    pool_scale,
    attention_out,
    pooling_out,
):
    length = query_rows.shape[0]
    heads = query_rows.shape[1] // HEAD
    group = pool_input.shape[1]
    width = attention_out.shape[1]
    half = width // 2
    cols = half // CHUNKS
    rows = length // n_tp
    gate_rows = log_gate_sums.T.reshape(-1, LANES)
    gate_rows = jnp.pad(gate_rows, ((0, -gate_rows.shape[0] % 8), (0, 0)))
    n_up = n_sp // 2
    n_down = max(n_sp - 1 - n_up, 1)
    vmem = pl.BlockSpec(memory_space=pltpu.VMEM)
    dma = pltpu.SemaphoreType.DMA
    return pl.pallas_call(
        functools.partial(kernel, n_sp, n_tp),
        out_shape=jax.ShapeDtypeStruct((rows, width), bf16),
        in_specs=[vmem] * 9 + [pl.BlockSpec(memory_space=pl.ANY)] * 2,
        out_specs=vmem,
        scratch_shapes=[
            pltpu.VMEM((n_sp, length, HEAD), bf16),
            pltpu.VMEM((n_sp, length, HEAD), bf16),
            pltpu.VMEM((n_sp,) + gate_rows.shape, f32),
            pltpu.VMEM((heads, length, HEAD), bf16),
            pltpu.VMEM((heads, length, LANES), f32),
            pltpu.VMEM((heads, length, LANES), f32),
            pltpu.VMEM((heads, length, HEAD), f32),
            pltpu.VMEM((4, length, group), bf16),
            pltpu.VMEM((MAX_WINDOW, group), bf16),
            pltpu.VMEM((2, heads * HEAD, half), bf16),
            pltpu.VMEM((2, group, half), bf16),
            pltpu.VMEM((length, half), f32),
            pltpu.VMEM((n_tp, CHUNKS, rows, cols), bf16),
            pltpu.VMEM((2, CHUNKS, rows, cols), bf16),
            pltpu.VMEM((3, 2, CHUNKS, rows, cols), bf16),
            dma((3, n_up)),
            dma((3, n_up)),
            dma((3, n_down)),
            dma((3, n_down)),
            dma((3,)),
            dma((3,)),
            dma((2,)),
            dma((2,)),
            dma((2,)),
            dma((2, CHUNKS)),
            dma((2, CHUNKS)),
            dma((3, 2, CHUNKS)),
            dma((3, 2, CHUNKS)),
        ],
        compiler_params=pltpu.CompilerParams(
            collective_id=0, has_side_effects=True, vmem_limit_bytes=56 * 1024 * 1024
        ),
    )(
        query_rows,
        key_rows,
        value_rows,
        gate_rows,
        pool_input,
        query_gain.reshape(1, -1),
        key_gain.reshape(1, -1),
        pool_weight,
        pool_scale.reshape(1, -1),
        attention_out,
        pooling_out,
    )


def solution(mesh):
    return jax.shard_map(
        functools.partial(body, mesh.shape["sp"], mesh.shape["tp"]),
        mesh=mesh,
        in_specs=(
            P(("grp", "sp"), "tp"),
            P(("grp", "sp"), "tp"),
            P(("grp", "sp"), "tp"),
            P(("grp", "sp"), "tp"),
            P(("grp", "sp"), "tp"),
            P(),
            P(),
            P("tp", None, None),
            P("tp"),
            P("tp", None),
            P("tp", None),
        ),
        out_specs=P(("grp", "sp", "tp"), None),
        check_vma=False,
    )
```

time: 318 us -> 145 us (0.46)
  the two profiles are of different devices: /device:TPU:1952 before, /device:TPU:33 now
where the time goes in v1:
time: 145 us
  Pallas kernels  142 us (98%)
  local copies, waits for them, and re-layouts  3.06 us (2%)
    pallas_call x1, Pallas kernels, body(): pl.pallas_call(functools.partial(kernel, n_sp, n_tp), out_shape=jax.Shape...  142 us

profile of v1, /device:TPU:33, one launch (start us, length us, event | category | flops | bytes accessed | tf_op | source)
XLA Modules:
  0.0 145.2 jit_solution(15611076588273301799)
XLA Ops:
  0.0 0.7 reshape.12
  0.7 0.6 pad.4.gate_ref
  1.3 142.2 %shard_map.109 = bf16[48,4096]{1,0:T(8,128)(2,1)} custom-call(bf16[384,256]{1,0:T(8,128)(2,1)} %q_ref.1, bf16[384,128]{1,0:T(8,128)(2,1)} %k_ref.1, bf16[384,128]{1,0:T(8,128)(2,1)} %v_ref.1, f32[8,128]{1,0:T(8,128)} %pad.4.gate_ref, bf16[384,256]{1,0:T(8,128)(2,1)} %pool_ref.1, f32[1,128]{1,0:T(1,128)} %bitcast.6, f32[1,128]{1,0:T(1,128)} %bitcast.7, ...), custom_call_target="tpu_custom_call" | custom-call | tf_op jit(solution)/shard_map/pallas_call | solution.py:478
  143.5 1.8 %copy.13 = bf16[48,4096]{1,0:T(8,128)(2,1)} copy(bf16[48,4096]{1,0:T(8,128)(2,1)} %shard_map.109) | data formatting | bytes 786432

commit v2 on v1

--- a/solution.py
+++ b/solution.py
@@ -12,6 +12,8 @@
 MAX_WINDOW = 16
 LANES = 128
 CHUNKS = 4
+WRAPPED = 13
+LAG = 3
 
 epsilon = 1e-06
 masked = -1e30
@@ -69,6 +71,7 @@
     up_recv,
     down_send,
     down_recv,
+    ready_sem,
     early_send,
     early_recv,
     local_sem,
@@ -93,8 +96,9 @@
     chip_far = lax.rem(chip + 2, n_x)
     above = lax.rem(me + 1, n_sp)
     below = lax.rem(me + n_sp - 1, n_sp)
-    n_up = n_sp // 2
-    n_down = n_sp - 1 - n_up
+    wrapped = min(WRAPPED, (n_sp - 1) // 2)
+    hops = n_sp - 1 - wrapped
+    last = n_sp - 1
     half = out_ref.shape[1] // 2
     cols = half // CHUNKS
     rows = out_ref.shape[0]
@@ -110,8 +114,13 @@
         )
 
     barrier = pltpu.get_barrier_semaphore()
+    @pl.when(me < last)
+    def _():
+        pl.semaphore_signal(
+            barrier, inc=1, device_id={"sp": above}, device_id_type=pl.DeviceIdType.MESH
+        )
+
     for where in (
-        {"sp": above},
         {"sp": below},
         {"tp": 2 * chip + other},
         {"tp": 2 * chip_right},
@@ -135,47 +144,52 @@
     keys[me] = normed(k_ref[...], k_gain_ref[...])
     values[me] = v_ref[...]
     gates[me] = gate_ref[...]
-
-    pl.semaphore_wait(barrier, 7)
-
-    def ring_copies(slot, step, src_first):
-        sources = (
-            (v_ref, gate_ref, keys.at[slot])
-            if src_first
-            else (values.at[slot], gates.at[slot], keys.at[slot])
-        )
-        targets = (values.at[slot], gates.at[slot], keys.at[slot])
-        return sources, targets
-
-    def up_copy(kind, slot, step, src_first=False):
-        sources, targets = ring_copies(slot, step, src_first)
+    for h in range(heads):
+        queries[h] = normed(q_ref[:, h * HEAD : (h + 1) * HEAD], q_gain_ref[...])
+
+    @pl.when(me == 0)
+    def _():
+        pl.semaphore_wait(barrier, 6)
+
+    @pl.when(me > 0)
+    def _():
+        pl.semaphore_wait(barrier, 7)
+
+    @pl.when(me == last)
+    def _():
+        pl.semaphore_signal(
+            ready_sem, inc=1, device_id={"sp": above}, device_id_type=pl.DeviceIdType.MESH
+        )
+
+    stores = (values, gates, keys)
+
+    def up_copy(kind, slot, step):
         return remote(
-            sources[kind],
-            targets[kind],
+            stores[kind].at[slot],
+            stores[kind].at[slot],
             up_send.at[kind, step],
             up_recv.at[kind, step],
             sp=above,
         )
 
-    def down_copy(kind, slot, step, src_first=False):
-        sources, targets = ring_copies(slot, step, src_first)
+    def down_copy(kind, slot):
         return remote(
-            sources[kind],
-            targets[kind],
-            down_send.at[kind, step],
-            down_recv.at[kind, step],
+            stores[kind].at[slot],
+            stores[kind].at[slot],
+            down_send.at[kind, slot],
+            down_recv.at[kind, slot],
             sp=below,
         )
 
-    for kind in (0, 1):
-        up_copy(kind, me, 0, True).start()
-        if n_down > 0:
-            down_copy(kind, me, 0, True).start()
-    for h in range(heads):
-        queries[h] = normed(q_ref[:, h * HEAD : (h + 1) * HEAD], q_gain_ref[...])
-    up_copy(2, me, 0, True).start()
-    if n_down > 0:
-        down_copy(2, me, 0, True).start()
+    @pl.when(me < last)
+    def _():
+        for kind in range(3):
+            up_copy(kind, me, 0).start()
+
+    @pl.when(jnp.logical_and(me > 0, me < wrapped))
+    def _():
+        for kind in range(3):
+            down_copy(kind, me).start()
 
     rim_copy = remote(
         pool_ref.at[pl.ds(length - MAX_WINDOW, MAX_WINDOW)],
@@ -198,7 +212,11 @@
         early_recv.at[2],
         tp=2 * chip + other,
     )
-    rim_copy.start()
+
+    @pl.when(me < last)
+    def _():
+        rim_copy.start()
+
     att_w_copy.start()
     pool_w_copy.start()
 
@@ -255,8 +273,15 @@
     level = lax.rem(tp, level_count)
 
     def pooling():
-        rim_copy.wait_recv()
-        edge = jnp.where(me > 0, rim[...].astype(f32), 0.0)
+        @pl.when(me == 0)
+        def _():
+            rim[...] = jnp.zeros_like(rim)
+
+        @pl.when(me > 0)
+        def _():
+            rim_copy.wait_recv()
+
+        edge = rim[...].astype(f32)
         here = pool_ref[...].astype(f32)
         window_sum = jnp.concatenate([edge, here], axis=0)
         chosen = jnp.zeros_like(here)
@@ -276,37 +301,52 @@
         mix.at[0], mix.at[1], mix_send.at[0], mix_recv.at[0], tp=partner
     )
 
+    low = me < wrapped
+    down_base = jnp.where(low, me - LAG, me - n_sp - 1)
+    down_first = jnp.where(low, me + 1, 0)
+    down_last = jnp.where(low, wrapped - 1, me - hops - 1)
+    up_steps = jnp.minimum(me, hops)
+
     def ring_step(step, carry):
-        slot_up = lax.rem(me - step + n_sp, n_sp)
-        slot_down = lax.rem(me + step, n_sp)
+        slot_up = jnp.maximum(me - step, 0)
+        slot_down = jnp.clip(down_base + step, 0, wrapped - 1)
+        takes_up = step <= up_steps
+        takes_down = jnp.logical_and(
+            down_base + step >= down_first, down_base + step <= down_last
+        )
         for kind in range(3):
-            up_copy(kind, slot_up, step - 1).wait_recv()
-
-            @pl.when(step < n_up)
+
+            @pl.when(takes_up)
+            def _():
+                up_copy(kind, slot_up, step - 1).wait_recv()
+
+            @pl.when(jnp.logical_and(takes_up, jnp.logical_and(step < hops, me < last)))
             def _():
                 up_copy(kind, slot_up, step).start()
 
-            if n_down > 0:
-
-                @pl.when(step <= n_down)
-                def _():
-                    down_copy(kind, slot_down, step - 1).wait_recv()
-
-                @pl.when(step < n_down)
-                def _():
-                    down_copy(kind, slot_down, step).start()
-
-        @pl.when(step <= me)
+            @pl.when(takes_down)
+            def _():
+                down_copy(kind, slot_down).wait_recv()
+
+            @pl.when(jnp.logical_and(takes_down, jnp.logical_or(low, slot_down < down_last)))
+            def _():
+                down_copy(kind, slot_down).start()
+
+        @pl.when(takes_up)
         def _():
             attend(slot_up)
 
-        @pl.when(jnp.logical_and(step <= n_down, me + step >= n_sp))
+        @pl.when(jnp.logical_and(takes_down, me > hops))
         def _():
             attend(slot_down)
 
         return carry
 
-    lax.fori_loop(1, 2, ring_step, 0)
+    steps = jnp.where(
+        me == 0, 0, jnp.maximum(up_steps, jnp.where(low, wrapped - 1 - me + LAG, 0))
+    )
+    first_steps = jnp.minimum(steps, 1)
+    lax.fori_loop(1, first_steps + 1, ring_step, 0)
 
     pool_mix_copy.start()
     load_att.wait()
@@ -318,7 +358,7 @@
         span = pl.ds(c * cols, cols)
         pool_part[:, span] = dot(mix[0], w_pool[0, :, span]) + dot(mix[1], w_pool[1, :, span])
 
-    lax.fori_loop(2, n_up + 1, ring_step, 0)
+    lax.fori_loop(first_steps + 1, steps + 1, ring_step, 0)
 
     for h in range(heads):
         weight_sum = jnp.sum(total[h], axis=-1, keepdims=True)
@@ -420,19 +460,38 @@
             first = source_core * half + c * cols
             out_ref[:, first : first + cols] = merged.astype(bf16)
 
-    def sent(step, carry):
+    @pl.when(me == 0)
+    def _():
+        pl.semaphore_wait(ready_sem, 1)
         for kind in range(3):
-            up_copy(kind, me, step).wait_send()
-            if n_down > 0:
-
-                @pl.when(step < n_down)
-                def _():
-                    down_copy(kind, me, step).wait_send()
-
+            down_copy(kind, 0).start()
+
+        def pass_on(slot, carry):
+            for kind in range(3):
+                down_copy(kind, slot).wait_recv()
+                down_copy(kind, slot).start()
+            return carry
+
+        lax.fori_loop(1, wrapped, pass_on, 0)
+
+    @pl.when(me < last)
+    def _():
+        def up_sent(step, carry):
+            for kind in range(3):
+                up_copy(kind, me, step).wait_send()
+            return carry
+
+        lax.fori_loop(0, jnp.minimum(me, hops - 1) + 1, up_sent, 0)
+        rim_copy.wait_send()
+
+    def down_sent(slot, carry):
+        for kind in range(3):
+            down_copy(kind, slot).wait_send()
         return carry
 
-    lax.fori_loop(0, n_up, sent, 0)
-    rim_copy.wait_send()
+    lax.fori_loop(
+        jnp.where(low, me, 0), jnp.where(low, wrapped, jnp.maximum(me - hops - 1, 0)), down_sent, 0
+    )
     att_w_copy.wait_send()
     pool_w_copy.wait_send()
     pool_mix_copy.wait_send()
@@ -471,8 +530,8 @@
     rows = length // n_tp
     gate_rows = log_gate_sums.T.reshape(-1, LANES)
     gate_rows = jnp.pad(gate_rows, ((0, -gate_rows.shape[0] % 8), (0, 0)))
-    n_up = n_sp // 2
-    n_down = max(n_sp - 1 - n_up, 1)
+    wrapped = min(WRAPPED, (n_sp - 1) // 2)
+    hops = n_sp - 1 - wrapped
     vmem = pl.BlockSpec(memory_space=pltpu.VMEM)
     dma = pltpu.SemaphoreType.DMA
     return pl.pallas_call(
@@ -496,10 +555,11 @@
             pltpu.VMEM((n_tp, CHUNKS, rows, cols), bf16),
             pltpu.VMEM((2, CHUNKS, rows, cols), bf16),
             pltpu.VMEM((3, 2, CHUNKS, rows, cols), bf16),
-            dma((3, n_up)),
-            dma((3, n_up)),
-            dma((3, n_down)),
-            dma((3, n_down)),
+            dma((3, hops)),
+            dma((3, hops)),
+            dma((3, wrapped)),
+            dma((3, wrapped)),
+            pltpu.SemaphoreType.REGULAR,
             dma((3,)),
             dma((3,)),
             dma((2,)),

time: 145 us -> 127 us (0.88)
  the two profiles are of different devices: /device:TPU:33 before, /device:TPU:37 now
where the time goes in v2:
time: 127 us
  Pallas kernels  124 us (98%)
  local copies, waits for them, and re-layouts  3.06 us (2%)
    pallas_call x1, Pallas kernels, body(): pl.pallas_call(functools.partial(kernel, n_sp, n_tp), out_shape=jax.Shape...  124 us

profile of v2, /device:TPU:37, one launch (start us, length us, event | category | flops | bytes accessed | tf_op | source)
XLA Modules:
  0.0 127.0 jit_solution(13251303936096947063)
XLA Ops:
  0.0 0.7 reshape.12
  0.7 0.6 pad.4.gate_ref
  1.3 123.9 %shard_map.109 = bf16[48,4096]{1,0:T(8,128)(2,1)} custom-call(bf16[384,256]{1,0:T(8,128)(2,1)} %q_ref.1, bf16[384,128]{1,0:T(8,128)(2,1)} %k_ref.1, bf16[384,128]{1,0:T(8,128)(2,1)} %v_ref.1, f32[8,128]{1,0:T(8,128)} %pad.4.gate_ref, bf16[384,256]{1,0:T(8,128)(2,1)} %pool_ref.1, f32[1,128]{1,0:T(1,128)} %bitcast.6, f32[1,128]{1,0:T(1,128)} %bitcast.7, ...), custom_call_target="tpu_custom_call" | custom-call | tf_op jit(solution)/shard_map/pallas_call | solution.py:537
  125.2 1.8 %copy.13 = bf16[48,4096]{1,0:T(8,128)(2,1)} copy(bf16[48,4096]{1,0:T(8,128)(2,1)} %shard_map.109) | data formatting | bytes 786432

commit v3 on v2

--- a/solution.py
+++ b/solution.py
@@ -12,8 +12,9 @@
 MAX_WINDOW = 16
 LANES = 128
 CHUNKS = 4
-WRAPPED = 13
-LAG = 3
+WRAPPED = 15
+AHEAD = 4
+SEND_STEP = 11
 
 epsilon = 1e-06
 masked = -1e30
@@ -120,6 +121,12 @@
             barrier, inc=1, device_id={"sp": above}, device_id_type=pl.DeviceIdType.MESH
         )
 
+    @pl.when(jnp.logical_and(me > 0, me < wrapped))
+    def _():
+        pl.semaphore_signal(
+            barrier, inc=1, device_id={"sp": last}, device_id_type=pl.DeviceIdType.MESH
+        )
+
     for where in (
         {"sp": below},
         {"tp": 2 * chip + other},
@@ -143,7 +150,15 @@
 
     keys[me] = normed(k_ref[...], k_gain_ref[...])
     values[me] = v_ref[...]
-    gates[me] = gate_ref[...]
+    gates[me] = jnp.concatenate(
+        [
+            gate_ref[h : h + 1, c * LANES : (c + 1) * LANES]
+            for h in range(heads)
+            for c in range(pieces)
+        ]
+        + [jnp.zeros((-(heads * pieces) % 8, LANES), f32)],
+        axis=0,
+    )
     for h in range(heads):
         queries[h] = normed(q_ref[:, h * HEAD : (h + 1) * HEAD], q_gain_ref[...])
 
@@ -151,15 +166,20 @@
     def _():
         pl.semaphore_wait(barrier, 6)
 
-    @pl.when(me > 0)
+    @pl.when(jnp.logical_and(me > 0, me < last))
     def _():
         pl.semaphore_wait(barrier, 7)
 
+    def let_send(plane):
+        pl.semaphore_signal(
+            ready_sem, inc=1, device_id={"sp": plane}, device_id_type=pl.DeviceIdType.MESH
+        )
+
     @pl.when(me == last)
     def _():
-        pl.semaphore_signal(
-            ready_sem, inc=1, device_id={"sp": above}, device_id_type=pl.DeviceIdType.MESH
-        )
+        pl.semaphore_wait(barrier, 6 + wrapped)
+        for plane in range(min(AHEAD, wrapped)):
+            let_send(plane)
 
     stores = (values, gates, keys)
 
@@ -172,24 +192,19 @@
             sp=above,
         )
 
-    def down_copy(kind, slot):
+    def down_copy(kind, slot, plane):
         return remote(
             stores[kind].at[slot],
             stores[kind].at[slot],
             down_send.at[kind, slot],
             down_recv.at[kind, slot],
-            sp=below,
+            sp=plane,
         )
 
     @pl.when(me < last)
     def _():
         for kind in range(3):
             up_copy(kind, me, 0).start()
-
-    @pl.when(jnp.logical_and(me > 0, me < wrapped))
-    def _():
-        for kind in range(3):
-            down_copy(kind, me).start()
 
     rim_copy = remote(
         pool_ref.at[pl.ds(length - MAX_WINDOW, MAX_WINDOW)],
@@ -224,7 +239,7 @@
 
     def score_pieces(h, slot):
         z = rows_dot(queries[h], keys[slot])
-        base = gate_ref[h * pieces : h * pieces + 1, 0:1]
+        base = gate_ref[h : h + 1, 0:1]
         lifted = (base - gates[slot]) * LOG2E
         return [
             z[:, c * LANES : (c + 1) * LANES] * scale
@@ -302,20 +317,27 @@
     )
 
     low = me < wrapped
-    down_base = jnp.where(low, me - LAG, me - n_sp - 1)
-    down_first = jnp.where(low, me + 1, 0)
-    down_last = jnp.where(low, wrapped - 1, me - hops - 1)
+    own_slot = jnp.minimum(me, wrapped - 1)
+    down_base = me - n_sp - 1
+    down_last = me - hops - 1
     up_steps = jnp.minimum(me, hops)
+    send_step = jnp.minimum(me, SEND_STEP)
+
+    def send_across():
+        pl.semaphore_wait(ready_sem, 1)
+        for kind in range(3):
+            down_copy(kind, own_slot, last).start()
+
+    def has_down(step):
+        return jnp.logical_and(down_base + step >= 0, down_base + step <= down_last)
 
     def ring_step(step, carry):
         slot_up = jnp.maximum(me - step, 0)
         slot_down = jnp.clip(down_base + step, 0, wrapped - 1)
         takes_up = step <= up_steps
-        takes_down = jnp.logical_and(
-            down_base + step >= down_first, down_base + step <= down_last
-        )
-        for kind in range(3):
-
+        takes_down = has_down(step)
+
+        def pass_on(kind):
             @pl.when(takes_up)
             def _():
                 up_copy(kind, slot_up, step - 1).wait_recv()
@@ -326,25 +348,41 @@
 
             @pl.when(takes_down)
             def _():
-                down_copy(kind, slot_down).wait_recv()
-
-            @pl.when(jnp.logical_and(takes_down, jnp.logical_or(low, slot_down < down_last)))
+                down_copy(kind, slot_down, below).wait_recv()
+
+            @pl.when(jnp.logical_and(takes_down, slot_down < down_last))
             def _():
-                down_copy(kind, slot_down).start()
-
-        @pl.when(takes_up)
+                down_copy(kind, slot_down, below).start()
+
+        pass_on(0)
+        pass_on(1)
+
+        @pl.when(jnp.logical_and(step > 1, step - 1 <= up_steps))
         def _():
-            attend(slot_up)
-
-        @pl.when(jnp.logical_and(takes_down, me > hops))
+            attend(jnp.maximum(me - step + 1, 0))
+
+        pass_on(2)
+
+        @pl.when(jnp.logical_and(me == last, takes_down))
         def _():
-            attend(slot_down)
+            for ahead in range(2):
+                plane = 2 * slot_down + AHEAD + ahead
+
+                @pl.when(plane < wrapped)
+                def _():
+                    let_send(plane)
+
+        @pl.when(has_down(step - 1))
+        def _():
+            attend(jnp.clip(down_base + step - 1, 0, wrapped - 1))
+
+        @pl.when(jnp.logical_and(low, step == send_step))
+        def _():
+            send_across()
 
         return carry
 
-    steps = jnp.where(
-        me == 0, 0, jnp.maximum(up_steps, jnp.where(low, wrapped - 1 - me + LAG, 0))
-    )
+    steps = jnp.where(me == 0, 0, up_steps + 1)
     first_steps = jnp.minimum(steps, 1)
     lax.fori_loop(1, first_steps + 1, ring_step, 0)
 
@@ -359,6 +397,10 @@
         pool_part[:, span] = dot(mix[0], w_pool[0, :, span]) + dot(mix[1], w_pool[1, :, span])
 
     lax.fori_loop(first_steps + 1, steps + 1, ring_step, 0)
+
+    @pl.when(me == 0)
+    def _():
+        send_across()
 
     for h in range(heads):
         weight_sum = jnp.sum(total[h], axis=-1, keepdims=True)
@@ -460,20 +502,6 @@
             first = source_core * half + c * cols
             out_ref[:, first : first + cols] = merged.astype(bf16)
 
-    @pl.when(me == 0)
-    def _():
-        pl.semaphore_wait(ready_sem, 1)
-        for kind in range(3):
-            down_copy(kind, 0).start()
-
-        def pass_on(slot, carry):
-            for kind in range(3):
-                down_copy(kind, slot).wait_recv()
-                down_copy(kind, slot).start()
-            return carry
-
-        lax.fori_loop(1, wrapped, pass_on, 0)
-
     @pl.when(me < last)
     def _():
         def up_sent(step, carry):
@@ -486,11 +514,14 @@
 
     def down_sent(slot, carry):
         for kind in range(3):
-            down_copy(kind, slot).wait_send()
+            down_copy(kind, slot, below).wait_send()
         return carry
 
     lax.fori_loop(
-        jnp.where(low, me, 0), jnp.where(low, wrapped, jnp.maximum(me - hops - 1, 0)), down_sent, 0
+        jnp.where(low, own_slot, 0),
+        jnp.where(low, own_slot + 1, jnp.maximum(me - hops - 1, 0)),
+        down_sent,
+        0,
     )
     att_w_copy.wait_send()
     pool_w_copy.wait_send()
@@ -528,8 +559,7 @@
     half = width // 2
     cols = half // CHUNKS
     rows = length // n_tp
-    gate_rows = log_gate_sums.T.reshape(-1, LANES)
-    gate_rows = jnp.pad(gate_rows, ((0, -gate_rows.shape[0] % 8), (0, 0)))
+    gate_tile = -(-heads * length // LANES // 8) * 8
     wrapped = min(WRAPPED, (n_sp - 1) // 2)
     hops = n_sp - 1 - wrapped
     vmem = pl.BlockSpec(memory_space=pltpu.VMEM)
@@ -542,7 +572,7 @@
         scratch_shapes=[
             pltpu.VMEM((n_sp, length, HEAD), bf16),
             pltpu.VMEM((n_sp, length, HEAD), bf16),
-            pltpu.VMEM((n_sp,) + gate_rows.shape, f32),
+            pltpu.VMEM((n_sp, gate_tile, LANES), f32),
             pltpu.VMEM((heads, length, HEAD), bf16),
             pltpu.VMEM((heads, length, LANES), f32),
             pltpu.VMEM((heads, length, LANES), f32),
@@ -577,7 +607,7 @@
         query_rows,
         key_rows,
         value_rows,
-        gate_rows,
+        log_gate_sums.T,
         pool_input,
         query_gain.reshape(1, -1),
         key_gain.reshape(1, -1),

time: 127 us -> 144 us (1.13)
  the two profiles are of different devices: /device:TPU:37 before, /device:TPU:1376 now
where the time goes in v3:
time: 144 us
  Pallas kernels  142 us (99%)
  local copies, waits for them, and re-layouts  1.77 us (1%)
    pallas_call x1, Pallas kernels, body(): pl.pallas_call(functools.partial(kernel, n_sp, n_tp), out_shape=jax.Shape...  142 us

profile of v3, /device:TPU:1376, one launch (start us, length us, event | category | flops | bytes accessed | tf_op | source)
XLA Modules:
  0.0 144.2 jit_solution(3829137200073085263)
XLA Ops:
  0.0 142.4 %shard_map.109 = bf16[48,4096]{1,0:T(8,128)(2,1)} custom-call(bf16[384,256]{1,0:T(8,128)(2,1)} %q_ref.1, bf16[384,128]{1,0:T(8,128)(2,1)} %k_ref.1, bf16[384,128]{1,0:T(8,128)(2,1)} %v_ref.1, f32[2,384]{1,0:T(2,128)} %bitcast.4, bf16[384,256]{1,0:T(8,128)(2,1)} %pool_ref.1, f32[1,128]{1,0:T(1,128)} %bitcast.6, f32[1,128]{1,0:T(1,128)} %bitcast.7, ...), custom_call_target="tpu_custom_call" | custom-call | tf_op jit(solution)/shard_map/pallas_call | solution.py:567
  142.5 1.8 %copy.13 = bf16[48,4096]{1,0:T(8,128)(2,1)} copy(bf16[48,4096]{1,0:T(8,128)(2,1)} %shard_map.109) | data formatting | bytes 786432

commit v4 on v2

--- a/solution.py
+++ b/solution.py
@@ -14,6 +14,9 @@
 CHUNKS = 4
 WRAPPED = 13
 LAG = 3
+UPPER_LAG = 3
+SOON_FIRST = 2
+SOON = 5
 
 epsilon = 1e-06
 masked = -1e30
@@ -72,6 +75,7 @@
     down_send,
     down_recv,
     ready_sem,
+    late_sem,
     early_send,
     early_recv,
     local_sem,
@@ -114,23 +118,35 @@
         )
 
     barrier = pltpu.get_barrier_semaphore()
-    @pl.when(me < last)
-    def _():
+    first = jnp.logical_and(me == 0, tp == 0)
+    beside_z = jnp.logical_and(tp == 0, me == 1)
+    beside_chip = jnp.logical_or(chip == 1, chip == n_x - 1)
+    beside_x = jnp.logical_and(me == 0, jnp.logical_or(tp == 1, beside_chip))
+    beside = jnp.logical_or(beside_z, beside_x)
+
+    def signal(sem, where):
         pl.semaphore_signal(
-            barrier, inc=1, device_id={"sp": above}, device_id_type=pl.DeviceIdType.MESH
-        )
-
-    for where in (
-        {"sp": below},
+            sem, inc=1, device_id=where, device_id_type=pl.DeviceIdType.MESH
+        )
+
+    neighbours = (
         {"tp": 2 * chip + other},
         {"tp": 2 * chip_right},
         {"tp": 2 * chip_right + 1},
         {"tp": 2 * chip_left},
         {"tp": 2 * chip_left + 1},
-    ):
-        pl.semaphore_signal(
-            barrier, inc=1, device_id=where, device_id_type=pl.DeviceIdType.MESH
-        )
+    )
+
+    signal(barrier, {"sp": below})
+
+    @pl.when(jnp.logical_not(first))
+    def _():
+        @pl.when(me < last)
+        def _():
+            signal(barrier, {"sp": above})
+
+        for where in neighbours:
+            signal(barrier, where)
 
     my_cols = pl.ds(pl.multiple_of(core * half, LANES), half)
     other_cols = pl.ds(pl.multiple_of(other * half, LANES), half)
@@ -143,23 +159,30 @@
 
     keys[me] = normed(k_ref[...], k_gain_ref[...])
     values[me] = v_ref[...]
-    gates[me] = gate_ref[...]
+    gates[me] = jnp.concatenate(
+        [
+            gate_ref[h : h + 1, c * LANES : (c + 1) * LANES]
+            for h in range(heads)
+            for c in range(pieces)
+        ]
+        + [jnp.zeros((-(heads * pieces) % 8, LANES), f32)],
+        axis=0,
+    )
     for h in range(heads):
         queries[h] = normed(q_ref[:, h * HEAD : (h + 1) * HEAD], q_gain_ref[...])
 
-    @pl.when(me == 0)
-    def _():
-        pl.semaphore_wait(barrier, 6)
-
-    @pl.when(me > 0)
-    def _():
-        pl.semaphore_wait(barrier, 7)
+    arrivals = 7 - jnp.where(me == 0, 1, 0) - jnp.where(beside, 1, 0)
+    pl.semaphore_wait(barrier, arrivals)
+
+    @pl.when(first)
+    def _():
+        signal(late_sem, {"sp": above})
+        for where in neighbours:
+            signal(late_sem, where)
 
     @pl.when(me == last)
     def _():
-        pl.semaphore_signal(
-            ready_sem, inc=1, device_id={"sp": above}, device_id_type=pl.DeviceIdType.MESH
-        )
+        signal(ready_sem, {"sp": above})
 
     stores = (values, gates, keys)
 
@@ -186,10 +209,15 @@
         for kind in range(3):
             up_copy(kind, me, 0).start()
 
-    @pl.when(jnp.logical_and(me > 0, me < wrapped))
-    def _():
+    def start_down():
         for kind in range(3):
             down_copy(kind, me).start()
+
+    starts_down = jnp.logical_and(me > 0, me < wrapped)
+
+    @pl.when(jnp.logical_and(starts_down, jnp.logical_not(beside)))
+    def _():
+        start_down()
 
     rim_copy = remote(
         pool_ref.at[pl.ds(length - MAX_WINDOW, MAX_WINDOW)],
@@ -217,14 +245,11 @@
     def _():
         rim_copy.start()
 
-    att_w_copy.start()
-    pool_w_copy.start()
-
     scale = LOG2E / math.sqrt(HEAD)
 
     def score_pieces(h, slot):
         z = rows_dot(queries[h], keys[slot])
-        base = gate_ref[h * pieces : h * pieces + 1, 0:1]
+        base = gate_ref[h : h + 1, 0:1]
         lifted = (base - gates[slot]) * LOG2E
         return [
             z[:, c * LANES : (c + 1) * LANES] * scale
@@ -296,26 +321,53 @@
         mix[0] = mixed.astype(bf16)
 
     pooling()
+
+    def cross(slot, carry):
+        for kind in range(3):
+            down_copy(kind, slot).wait_recv()
+            down_copy(kind, slot).start()
+        return carry
+
+    soon = jnp.where(first, SOON_FIRST, SOON)
+
+    @pl.when(me == 0)
+    def _():
+        pl.semaphore_wait(ready_sem, 1)
+        for kind in range(3):
+            down_copy(kind, 0).start()
+        lax.fori_loop(1, soon, cross, 0)
+
+    @pl.when(beside)
+    def _():
+        pl.semaphore_wait(late_sem, 1)
+
+        @pl.when(starts_down)
+        def _():
+            start_down()
+
+    att_w_copy.start()
+    pool_w_copy.start()
     partner = 2 * chip + other
     pool_mix_copy = remote(
         mix.at[0], mix.at[1], mix_send.at[0], mix_recv.at[0], tp=partner
     )
 
     low = me < wrapped
-    down_base = jnp.where(low, me - LAG, me - n_sp - 1)
+    down_base = jnp.where(low, me - LAG, me - n_sp + 1 - UPPER_LAG)
     down_first = jnp.where(low, me + 1, 0)
     down_last = jnp.where(low, wrapped - 1, me - hops - 1)
     up_steps = jnp.minimum(me, hops)
+
+    def has_down(step):
+        return jnp.logical_and(down_base + step >= down_first, down_base + step <= down_last)
 
     def ring_step(step, carry):
         slot_up = jnp.maximum(me - step, 0)
         slot_down = jnp.clip(down_base + step, 0, wrapped - 1)
         takes_up = step <= up_steps
-        takes_down = jnp.logical_and(
-            down_base + step >= down_first, down_base + step <= down_last
-        )
-        for kind in range(3):
-
+        takes_down = has_down(step)
+
+        def pass_on(kind):
             @pl.when(takes_up)
             def _():
                 up_copy(kind, slot_up, step - 1).wait_recv()
@@ -332,18 +384,23 @@
             def _():
                 down_copy(kind, slot_down).start()
 
-        @pl.when(takes_up)
+        pass_on(0)
+        pass_on(1)
+
+        @pl.when(jnp.logical_and(step > 1, step - 1 <= up_steps))
         def _():
-            attend(slot_up)
-
-        @pl.when(jnp.logical_and(takes_down, me > hops))
+            attend(jnp.maximum(me - step + 1, 0))
+
+        pass_on(2)
+
+        @pl.when(jnp.logical_and(me > hops, has_down(step - 1)))
         def _():
-            attend(slot_down)
+            attend(jnp.clip(down_base + step - 1, 0, wrapped - 1))
 
         return carry
 
     steps = jnp.where(
-        me == 0, 0, jnp.maximum(up_steps, jnp.where(low, wrapped - 1 - me + LAG, 0))
+        me == 0, 0, jnp.maximum(up_steps + 1, jnp.where(low, wrapped - 1 - me + LAG, 0))
     )
     first_steps = jnp.minimum(steps, 1)
     lax.fori_loop(1, first_steps + 1, ring_step, 0)
@@ -365,6 +422,9 @@
         mix[2, :, h * HEAD : (h + 1) * HEAD] = (acc[h] / weight_sum).astype(bf16)
     att_mix_copy = remote(mix.at[2], mix.at[3], mix_send.at[1], mix_recv.at[1], tp=partner)
     att_mix_copy.start()
+    for c in range(CHUNKS):
+        span = pl.ds(c * cols, cols)
+        pool_part[:, span] += dot(mix[2], w_att[0, :, span])
     att_mix_copy.wait_recv()
 
     def relay_copies(c):
@@ -406,11 +466,7 @@
 
     for c in range(CHUNKS):
         span = pl.ds(c * cols, cols)
-        part = (
-            dot(mix[2], w_att[0, :, span])
-            + dot(mix[3], w_att[1, :, span])
-            + pool_part[:, span]
-        ).astype(bf16)
+        part = (pool_part[:, span] + dot(mix[3], w_att[1, :, span])).astype(bf16)
         for d in range(n_tp):
             parts[d, c] = part[d * rows : (d + 1) * rows]
         for copy in relay_copies(c):
@@ -418,6 +474,11 @@
     for c in range(CHUNKS):
         land_copy(0, chip_right, 1, c).start()
         land_copy(1, chip_left, 0, c).start()
+
+    @pl.when(me == 0)
+    def _():
+        cross(soon, 0)
+
     for c in range(CHUNKS):
         home_copy(c).start()
     for c in range(CHUNKS):
@@ -431,6 +492,10 @@
             parts[target, c] = joined.astype(bf16)
         land_copy(0, chip_right, 0, c).start()
         land_copy(1, chip_left, 1, c).start()
+
+        @pl.when(me == 0)
+        def _():
+            cross(soon + 1 + c, 0)
 
     def landed_wait(side, source_core, c):
         remote(
@@ -462,17 +527,7 @@
 
     @pl.when(me == 0)
     def _():
-        pl.semaphore_wait(ready_sem, 1)
-        for kind in range(3):
-            down_copy(kind, 0).start()
-
-        def pass_on(slot, carry):
-            for kind in range(3):
-                down_copy(kind, slot).wait_recv()
-                down_copy(kind, slot).start()
-            return carry
-
-        lax.fori_loop(1, wrapped, pass_on, 0)
+        lax.fori_loop(soon + 1 + CHUNKS, wrapped, cross, 0)
 
     @pl.when(me < last)
     def _():
@@ -490,7 +545,10 @@
         return carry
 
     lax.fori_loop(
-        jnp.where(low, me, 0), jnp.where(low, wrapped, jnp.maximum(me - hops - 1, 0)), down_sent, 0
+        jnp.where(low, me, 0),
+        jnp.where(low, wrapped, jnp.maximum(me - hops - 1, 0)),
+        down_sent,
+        0,
     )
     att_w_copy.wait_send()
     pool_w_copy.wait_send()
@@ -528,8 +586,7 @@
     half = width // 2
     cols = half // CHUNKS
     rows = length // n_tp
-    gate_rows = log_gate_sums.T.reshape(-1, LANES)
-    gate_rows = jnp.pad(gate_rows, ((0, -gate_rows.shape[0] % 8), (0, 0)))
+    gate_tile = -(-heads * length // LANES // 8) * 8
     wrapped = min(WRAPPED, (n_sp - 1) // 2)
     hops = n_sp - 1 - wrapped
     vmem = pl.BlockSpec(memory_space=pltpu.VMEM)
@@ -542,7 +599,7 @@
         scratch_shapes=[
             pltpu.VMEM((n_sp, length, HEAD), bf16),
             pltpu.VMEM((n_sp, length, HEAD), bf16),
-            pltpu.VMEM((n_sp,) + gate_rows.shape, f32),
+            pltpu.VMEM((n_sp, gate_tile, LANES), f32),
             pltpu.VMEM((heads, length, HEAD), bf16),
             pltpu.VMEM((heads, length, LANES), f32),
             pltpu.VMEM((heads, length, LANES), f32),
@@ -559,6 +616,7 @@
             dma((3, hops)),
             dma((3, wrapped)),
             dma((3, wrapped)),
+            pltpu.SemaphoreType.REGULAR,
             pltpu.SemaphoreType.REGULAR,
             dma((3,)),
             dma((3,)),
@@ -577,7 +635,7 @@
         query_rows,
         key_rows,
         value_rows,
-        gate_rows,
+        log_gate_sums.T,
         pool_input,
         query_gain.reshape(1, -1),
         key_gain.reshape(1, -1),

time: 127 us -> 117 us (0.921)
  the two profiles are of different devices: /device:TPU:37 before, /device:TPU:1570 now
where the time goes in v4:
time: 117 us
  Pallas kernels  115 us (98%)
  local copies, waits for them, and re-layouts  1.77 us (2%)
    pallas_call x1, Pallas kernels, body(): pl.pallas_call(functools.partial(kernel, n_sp, n_tp), out_shape=jax.Shape...  115 us

profile of v4, /device:TPU:1570, one launch (start us, length us, event | category | flops | bytes accessed | tf_op | source)
XLA Modules:
  0.0 117.1 jit_solution(9129610679555274046)
XLA Ops:
  0.0 115.3 %shard_map.109 = bf16[48,4096]{1,0:T(8,128)(2,1)} custom-call(bf16[384,256]{1,0:T(8,128)(2,1)} %q_ref.1, bf16[384,128]{1,0:T(8,128)(2,1)} %k_ref.1, bf16[384,128]{1,0:T(8,128)(2,1)} %v_ref.1, f32[2,384]{1,0:T(2,128)} %bitcast.4, bf16[384,256]{1,0:T(8,128)(2,1)} %pool_ref.1, f32[1,128]{1,0:T(1,128)} %bitcast.6, f32[1,128]{1,0:T(1,128)} %bitcast.7, ...), custom_call_target="tpu_custom_call" | custom-call | tf_op jit(solution)/shard_map/pallas_call | solution.py:594
  115.3 1.8 %copy.13 = bf16[48,4096]{1,0:T(8,128)(2,1)} copy(bf16[48,4096]{1,0:T(8,128)(2,1)} %shard_map.109) | data formatting | bytes 786432

commit v5 on v4

--- a/solution.py
+++ b/solution.py
@@ -14,9 +14,12 @@
 CHUNKS = 4
 WRAPPED = 13
 LAG = 3
-UPPER_LAG = 3
-SOON_FIRST = 2
-SOON = 5
+LAST_LAG = 3
+UPPER_LAG = 5
+SOON_FIRST = 1
+SOON = 7
+POOL_AFTER = 1
+PROJECT_AFTER = 3
 
 epsilon = 1e-06
 masked = -1e30
@@ -204,21 +207,6 @@
             sp=below,
         )
 
-    @pl.when(me < last)
-    def _():
-        for kind in range(3):
-            up_copy(kind, me, 0).start()
-
-    def start_down():
-        for kind in range(3):
-            down_copy(kind, me).start()
-
-    starts_down = jnp.logical_and(me > 0, me < wrapped)
-
-    @pl.when(jnp.logical_and(starts_down, jnp.logical_not(beside)))
-    def _():
-        start_down()
-
     rim_copy = remote(
         pool_ref.at[pl.ds(length - MAX_WINDOW, MAX_WINDOW)],
         rim,
@@ -226,6 +214,22 @@
         early_recv.at[0],
         sp=above,
     )
+    @pl.when(me < last)
+    def _():
+        rim_copy.start()
+        for kind in range(3):
+            up_copy(kind, me, 0).start()
+
+    def start_down():
+        for kind in range(3):
+            down_copy(kind, me).start()
+
+    starts_down = jnp.logical_and(me > 0, me < wrapped)
+
+    @pl.when(jnp.logical_and(starts_down, jnp.logical_not(beside)))
+    def _():
+        start_down()
+
     att_w_copy = remote(
         att_w_hbm.at[:, other_cols],
         w_att.at[1],
@@ -240,11 +244,6 @@
         early_recv.at[2],
         tp=2 * chip + other,
     )
-
-    @pl.when(me < last)
-    def _():
-        rim_copy.start()
-
     scale = LOG2E / math.sqrt(HEAD)
 
     def score_pieces(h, slot):
@@ -320,8 +319,6 @@
         mixed = dot(pooled, pool_w_ref[0]) * pool_s_ref[...]
         mix[0] = mixed.astype(bf16)
 
-    pooling()
-
     def cross(slot, carry):
         for kind in range(3):
             down_copy(kind, slot).wait_recv()
@@ -353,7 +350,8 @@
     )
 
     low = me < wrapped
-    down_base = jnp.where(low, me - LAG, me - n_sp + 1 - UPPER_LAG)
+    down_lag = jnp.where(me == last, LAST_LAG, UPPER_LAG)
+    down_base = jnp.where(low, me - LAG, me - n_sp + 1 - down_lag)
     down_first = jnp.where(low, me + 1, 0)
     down_last = jnp.where(low, wrapped - 1, me - hops - 1)
     up_steps = jnp.minimum(me, hops)
@@ -402,10 +400,13 @@
     steps = jnp.where(
         me == 0, 0, jnp.maximum(up_steps + 1, jnp.where(low, wrapped - 1 - me + LAG, 0))
     )
-    first_steps = jnp.minimum(steps, 1)
-    lax.fori_loop(1, first_steps + 1, ring_step, 0)
-
+    pool_step = jnp.minimum(steps, POOL_AFTER)
+    project_step = jnp.minimum(steps, PROJECT_AFTER)
+    lax.fori_loop(1, pool_step + 1, ring_step, 0)
+    pooling()
     pool_mix_copy.start()
+    lax.fori_loop(pool_step + 1, project_step + 1, ring_step, 0)
+
     load_att.wait()
     load_pool.wait()
     att_w_copy.wait_recv()
@@ -415,7 +416,11 @@
         span = pl.ds(c * cols, cols)
         pool_part[:, span] = dot(mix[0], w_pool[0, :, span]) + dot(mix[1], w_pool[1, :, span])
 
-    lax.fori_loop(first_steps + 1, steps + 1, ring_step, 0)
+    @pl.when(me == 0)
+    def _():
+        cross(soon, 0)
+
+    lax.fori_loop(project_step + 1, steps + 1, ring_step, 0)
 
     for h in range(heads):
         weight_sum = jnp.sum(total[h], axis=-1, keepdims=True)
@@ -477,7 +482,7 @@
 
     @pl.when(me == 0)
     def _():
-        cross(soon, 0)
+        cross(soon + 1, 0)
 
     for c in range(CHUNKS):
         home_copy(c).start()
@@ -495,7 +500,7 @@
 
         @pl.when(me == 0)
         def _():
-            cross(soon + 1 + c, 0)
+            cross(soon + 2 + c, 0)
 
     def landed_wait(side, source_core, c):
         remote(
@@ -527,7 +532,7 @@
 
     @pl.when(me == 0)
     def _():
-        lax.fori_loop(soon + 1 + CHUNKS, wrapped, cross, 0)
+        lax.fori_loop(soon + 2 + CHUNKS, wrapped, cross, 0)
 
     @pl.when(me < last)
     def _():

time: 117 us -> 117 us (level)
  no operation moved by 1% of the time
where the time goes in v5:
time: 117 us
  Pallas kernels  115 us (98%)
  local copies, waits for them, and re-layouts  1.77 us (2%)
    pallas_call x1, Pallas kernels, body(): pl.pallas_call(functools.partial(kernel, n_sp, n_tp), out_shape=jax.Shape...  115 us

profile of v5, /device:TPU:1570, one launch (start us, length us, event | category | flops | bytes accessed | tf_op | source)
XLA Modules:
  0.0 116.5 jit_solution(1542317982284419272)
XLA Ops:
  0.0 114.8 %shard_map.109 = bf16[48,4096]{1,0:T(8,128)(2,1)} custom-call(bf16[384,256]{1,0:T(8,128)(2,1)} %q_ref.1, bf16[384,128]{1,0:T(8,128)(2,1)} %k_ref.1, bf16[384,128]{1,0:T(8,128)(2,1)} %v_ref.1, f32[2,384]{1,0:T(2,128)} %bitcast.4, bf16[384,256]{1,0:T(8,128)(2,1)} %pool_ref.1, f32[1,128]{1,0:T(1,128)} %bitcast.6, f32[1,128]{1,0:T(1,128)} %bitcast.7, ...), custom_call_target="tpu_custom_call" | custom-call | tf_op jit(solution)/shard_map/pallas_call | solution.py:599
  114.8 1.8 %copy.13 = bf16[48,4096]{1,0:T(8,128)(2,1)} copy(bf16[48,4096]{1,0:T(8,128)(2,1)} %shard_map.109) | data formatting | bytes 786432

commit v6 on v5

--- a/solution.py
+++ b/solution.py
@@ -15,9 +15,10 @@
 WRAPPED = 13
 LAG = 3
 LAST_LAG = 3
-UPPER_LAG = 5
+NEAR_LAG = 5
+UPPER_LAG = 6
 SOON_FIRST = 1
-SOON = 7
+SOON = 4
 POOL_AFTER = 1
 PROJECT_AFTER = 3
 
@@ -332,7 +333,6 @@
         pl.semaphore_wait(ready_sem, 1)
         for kind in range(3):
             down_copy(kind, 0).start()
-        lax.fori_loop(1, soon, cross, 0)
 
     @pl.when(beside)
     def _():
@@ -344,13 +344,20 @@
 
     att_w_copy.start()
     pool_w_copy.start()
+
+    @pl.when(me == 0)
+    def _():
+        lax.fori_loop(1, soon, cross, 0)
+
     partner = 2 * chip + other
     pool_mix_copy = remote(
         mix.at[0], mix.at[1], mix_send.at[0], mix_recv.at[0], tp=partner
     )
 
     low = me < wrapped
-    down_lag = jnp.where(me == last, LAST_LAG, UPPER_LAG)
+    down_lag = jnp.where(
+        me == last, LAST_LAG, jnp.where(me >= last - 2, NEAR_LAG, UPPER_LAG)
+    )
     down_base = jnp.where(low, me - LAG, me - n_sp + 1 - down_lag)
     down_first = jnp.where(low, me + 1, 0)
     down_last = jnp.where(low, wrapped - 1, me - hops - 1)
@@ -401,7 +408,7 @@
         me == 0, 0, jnp.maximum(up_steps + 1, jnp.where(low, wrapped - 1 - me + LAG, 0))
     )
     pool_step = jnp.minimum(steps, POOL_AFTER)
-    project_step = jnp.minimum(steps, PROJECT_AFTER)
+    project_step = jnp.where(low, steps, jnp.minimum(steps, PROJECT_AFTER))
     lax.fori_loop(1, pool_step + 1, ring_step, 0)
     pooling()
     pool_mix_copy.start()

time: 117 us -> 115 us (0.983)
  the two profiles are of different devices: /device:TPU:1570 before, /device:TPU:1312 now
where the time goes in v6:
time: 115 us
  Pallas kernels  113 us (98%)
  local copies, waits for them, and re-layouts  1.77 us (2%)
    pallas_call x1, Pallas kernels, body(): pl.pallas_call(functools.partial(kernel, n_sp, n_tp), out_shape=jax.Shape...  113 us

profile of v6, /device:TPU:1312, one launch (start us, length us, event | category | flops | bytes accessed | tf_op | source)
XLA Modules:
  0.0 115.2 jit_solution(16856571963795114530)
XLA Ops:
  0.0 113.4 %shard_map.109 = bf16[48,4096]{1,0:T(8,128)(2,1)} custom-call(bf16[384,256]{1,0:T(8,128)(2,1)} %q_ref.1, bf16[384,128]{1,0:T(8,128)(2,1)} %k_ref.1, bf16[384,128]{1,0:T(8,128)(2,1)} %v_ref.1, f32[2,384]{1,0:T(2,128)} %bitcast.4, bf16[384,256]{1,0:T(8,128)(2,1)} %pool_ref.1, f32[1,128]{1,0:T(1,128)} %bitcast.6, f32[1,128]{1,0:T(1,128)} %bitcast.7, ...), custom_call_target="tpu_custom_call" | custom-call | tf_op jit(solution)/shard_map/pallas_call | solution.py:606
  113.5 1.8 %copy.13 = bf16[48,4096]{1,0:T(8,128)(2,1)} copy(bf16[48,4096]{1,0:T(8,128)(2,1)} %shard_map.109) | data formatting | bytes 786432

commit v7 on v6

--- a/solution.py
+++ b/solution.py
@@ -13,10 +13,10 @@
 LANES = 128
 CHUNKS = 4
 WRAPPED = 13
-LAG = 3
+LAG = 2
 LAST_LAG = 3
-NEAR_LAG = 5
-UPPER_LAG = 6
+UPPER_LAG = 4
+DRIFT = 6
 SOON_FIRST = 1
 SOON = 4
 POOL_AFTER = 1
@@ -356,7 +356,7 @@
 
     low = me < wrapped
     down_lag = jnp.where(
-        me == last, LAST_LAG, jnp.where(me >= last - 2, NEAR_LAG, UPPER_LAG)
+        me == last, LAST_LAG, UPPER_LAG + lax.div(last - me, DRIFT)
     )
     down_base = jnp.where(low, me - LAG, me - n_sp + 1 - down_lag)
     down_first = jnp.where(low, me + 1, 0)

time: 115 us -> 112 us (0.974)
  the two profiles are of different devices: /device:TPU:1312 before, /device:TPU:98 now
where the time goes in v7:
time: 112 us; the launch traced here: 111 us
  Pallas kernels  110 us (98%)
  local copies, waits for them, and re-layouts  1.77 us (2%)
    pallas_call x1, Pallas kernels, body(): pl.pallas_call(functools.partial(kernel, n_sp, n_tp), out_shape=jax.Shape...  110 us

profile of v7, /device:TPU:98, one launch (start us, length us, event | category | flops | bytes accessed | tf_op | source)
XLA Modules:
  0.0 111.5 jit_solution(8722691744317416695)
XLA Ops:
  0.0 109.7 %shard_map.109 = bf16[48,4096]{1,0:T(8,128)(2,1)} custom-call(bf16[384,256]{1,0:T(8,128)(2,1)} %q_ref.1, bf16[384,128]{1,0:T(8,128)(2,1)} %k_ref.1, bf16[384,128]{1,0:T(8,128)(2,1)} %v_ref.1, f32[2,384]{1,0:T(2,128)} %bitcast.4, bf16[384,256]{1,0:T(8,128)(2,1)} %pool_ref.1, f32[1,128]{1,0:T(1,128)} %bitcast.6, f32[1,128]{1,0:T(1,128)} %bitcast.7, ...), custom_call_target="tpu_custom_call" | custom-call | tf_op jit(solution)/shard_map/pallas_call | solution.py:606
  109.7 1.8 %copy.13 = bf16[48,4096]{1,0:T(8,128)(2,1)} copy(bf16[48,4096]{1,0:T(8,128)(2,1)} %shard_map.109) | data formatting | bytes 786432
